TPU v7x, 512 devices: a whole 4x8x8 slice. The times are simulated.
512 devices in a mesh: sp: 128 (over z, y, core), tp: 4 (over x).
Axes of the slice: x: 4, y: 8, z: 8, core: 2. Of those that a mesh axis runs over, the one named last changes fastest.
Arguments:
- glu_value: bfloat16 [131072, 1024], P('sp', 'tp'), may hold values from -6 to 6
- glu_gate: bfloat16 [131072, 1024], P('sp', 'tp'), may hold values from -8 to 8
- conv_taps: float32 [31, 1024], P(None, 'tp'), may hold values from -1 to 1
- channel_gain: float32 [1024], P('tp'), may hold values from 0.1 to 1.9
- proj_weight: bfloat16 [1024, 1024], P('tp'), may hold values from -0.1875 to 0.1875
- out_grad: bfloat16 [131072, 1024], P('sp'), may hold values from -6 to 6
Outputs:
- value_grad: bfloat16 [131072, 1024], P('sp', 'tp')
- gate_grad: bfloat16 [131072, 1024], P('sp', 'tp')
- proj_grad: float32 [1024, 1024], P(('tp', 'sp'))
- taps_grad: float32 [31, 1024], P(None, 'tp')
- norm_gain_gradient: float32 [1024], P('tp')
All inputs are finite; a program needn't handle non-finite values.
Results may differ from a plain program's by a relative error of at most 0.0029.
Values may be sent and summed in bfloat16 or wider, within the bound.
A program may use at most 64 MiB of HBM per device.

v0:
```python
import jax
import jax.numpy as jnp
from jax import lax
from jax.sharding import Mesh
from jax.sharding import PartitionSpec as P

SP = ("sp_0", "sp_1", "sp_2")
TP_SP = ("tp", "sp_0", "sp_1", "sp_2")


def from_behind(block, axis, distance):
    devices = range(lax.axis_size(axis))
    route = [(i - distance, i) for i in devices if i - distance in devices]
    return lax.ppermute(block, axis, route)


def sent_to_all(array, axis):
    peers = lax.axis_size(axis)
    return lax.all_to_all(
        jnp.broadcast_to(array[None], (peers, *array.shape)), axis, 0, 0, tiled=True
    )


def over_copies(array, axis):
    everything = sent_to_all(array, axis)
    return jnp.sum(everything, axis=0)


def together(arrays, axis):
    ends = [0]
    for a in arrays:
        ends.append(ends[-1] + a.size)
    so_far = over_copies(jnp.concatenate([a.ravel() for a in arrays]), axis)
    return tuple((so_far[b:e].reshape(a.shape) for a, b, e in zip(arrays, ends, ends[1:])))


def in_blocks(array, dim, peers):
    before, after = (array.shape[:dim], array.shape[dim + 1 :])
    return jnp.moveaxis(array.reshape(*before, peers, -1, *after), dim, 0)


def sent_and_summed(array, axis, dim):
    peers = lax.axis_size(axis)
    tiles = lax.all_to_all(in_blocks(array, dim, peers), axis, 0, 0, tiled=True)
    return jnp.sum(tiles, axis=0)


def sum_by_axis(array, axes, dim):
    far, near = axes
    own = sent_and_summed(in_blocks(array, dim, lax.axis_size(far)), near, dim + 1)
    return jnp.sum(lax.all_to_all(own, far, 0, 0, tiled=True), axis=0)


def rows_for(lines, peers):
    spare = -lines.shape[0] % peers
    if not spare:
        return lines
    return jnp.concatenate([lines, jnp.zeros((spare, *lines.shape[1:]), lines.dtype)])


def laid_out(tiles, dim):
    shape = list(tiles.shape[1:])
    shape[dim] *= tiles.shape[0]
    return jnp.moveaxis(tiles, 0, dim).reshape(shape)


def gathered_by_axis(array, axes, dim):
    far, near = axes
    initial = sent_to_all(array, far)
    tiles = jnp.swapaxes(sent_to_all(initial, near), 0, 1)
    return laid_out(tiles.reshape(-1, *array.shape), dim)


def nested_sum(array, axes):
    padded = rows_for(array, lax.axis_size(axes[0]) * lax.axis_size(axes[1]))
    whole = gathered_by_axis(sum_by_axis(padded, axes, 0), axes, 0)
    return lax.slice_in_dim(whole, 0, len(array)).reshape(array.shape)


def packed_total(arrays, axis):
    flat, at, done = (jnp.concatenate([a.reshape(-1) for a in arrays]), 0, [])
    so_far = nested_sum(flat, axis)
    for a in arrays:
        done.append(so_far[at : at + a.size].reshape(a.shape))
        at += a.size
    return tuple(done)


def per_device(glu_value, glu_gate, conv_taps, channel_gain, proj_weight, out_grad):
    kernel_len = conv_taps.shape[0]
    halo_rows = kernel_len - 1
    row_count = glu_value.shape[0]
    channel_width = channel_gain.shape[0] * lax.axis_size("tp")
    gradient_factor = 1.0 / jnp.sqrt(jnp.float32(row_count * lax.axis_size(SP)))
    prev_value, prev_gate = from_behind(
        (glu_value[row_count - halo_rows :], glu_gate[row_count - halo_rows :]), SP, 1
    )
    value_ext = jnp.concatenate([prev_value, glu_value], axis=0)
    gate_ext = jnp.concatenate([prev_gate, glu_gate], axis=0)
    glu_out = value_ext.astype(jnp.float32) * jax.nn.sigmoid(gate_ext.astype(jnp.float32))
    convolved_output = jnp.zeros((row_count, glu_out.shape[1]), jnp.float32)
    for tap in range(kernel_len):
        convolved_output = convolved_output + conv_taps[tap] * glu_out[tap : tap + row_count]
    row_sum, row_sq = together(
        (jnp.sum(convolved_output, axis=1), jnp.sum(convolved_output * convolved_output, axis=1)),
        "tp",
    )
    row_average = (row_sum / channel_width)[:, None]
    inverse_deviation = lax.rsqrt(
        (row_sq / channel_width)[:, None] - row_average * row_average + 1e-05
    )
    centered_scaled = (convolved_output - row_average) * inverse_deviation
    normalized_rows = centered_scaled * channel_gain
    activ = jax.nn.silu(normalized_rows).astype(jnp.bfloat16)
    act_grad = lax.dot_general(
        out_grad, proj_weight, (((1,), (1,)), ((), ())), preferred_element_type=jnp.float32
    )
    norm_sig = jax.nn.sigmoid(normalized_rows)
    normalized_gradient = act_grad * norm_sig * (1.0 + normalized_rows * (1.0 - norm_sig))
    centered_scaled_gradient = normalized_gradient * channel_gain
    backward_first, backward_second = together(
        (
            jnp.sum(centered_scaled_gradient, axis=1),
            jnp.sum(centered_scaled_gradient * centered_scaled, axis=1),
        ),
        "tp",
    )
    convolved_gradient = inverse_deviation * (
        centered_scaled_gradient
        - (backward_first / channel_width)[:, None]
        - centered_scaled * (backward_second / channel_width)[:, None]
    )
    gain_product = jnp.sum(normalized_gradient * centered_scaled, axis=0) * gradient_factor
    taps_term = (
        jnp.stack(
            [
                jnp.sum(convolved_gradient * glu_out[tap : tap + row_count], axis=0)
                for tap in range(kernel_len)
            ]
        )
        * gradient_factor
    )
    zero_rows = jnp.zeros((halo_rows, glu_out.shape[1]), jnp.float32)
    grad_pad = jnp.concatenate([zero_rows, convolved_gradient, zero_rows], axis=0)
    grad_ext = jnp.zeros((row_count + halo_rows, glu_out.shape[1]), jnp.float32)
    for tap in range(kernel_len):
        grad_ext = (
            grad_ext
            + conv_taps[tap] * grad_pad[halo_rows - tap : halo_rows - tap + row_count + halo_rows]
        )
    returned = from_behind(grad_ext[:halo_rows], SP, -1)
    own_part = grad_ext[halo_rows:]
    glu_grad = jnp.concatenate(
        [own_part[: row_count - halo_rows], own_part[row_count - halo_rows :] + returned], axis=0
    )
    value_f = glu_value.astype(jnp.float32)
    gate_sig = jax.nn.sigmoid(glu_gate.astype(jnp.float32))
    value_grad = (glu_grad * gate_sig).astype(jnp.bfloat16)
    gate_grad = (glu_grad * value_f * gate_sig * (1.0 - gate_sig)).astype(jnp.bfloat16)
    proj_grad = sum_by_axis(
        lax.dot_general(
            activ, out_grad, (((0,), (0,)), ((), ())), preferred_element_type=jnp.float32
        )
        * gradient_factor,
        (("sp_0", "sp_1"), "sp_2"),
        0,
    )
    taps_grad, norm_gain_gradient = packed_total(
        (taps_term, gain_product), (("sp_0", "sp_1"), "sp_2")
    )
    return (value_grad, gate_grad, proj_grad, taps_grad, norm_gain_gradient)


def solution(mesh):
    finer = Mesh(mesh.devices.reshape(8, 8, 2, mesh.shape["tp"]), ("sp_0", "sp_1", "sp_2", "tp"))
    return jax.shard_map(
        per_device,
        mesh=finer,
        in_specs=(P(SP, "tp"), P(SP, "tp"), P(None, "tp"), P("tp"), P("tp", None), P(SP, None)),
        out_specs=(P(SP, "tp"), P(SP, "tp"), P(TP_SP, None), P(None, "tp"), P("tp")),
        check_vma=False,
    )
```

profile of v0, /device:TPU:1, one launch (start us, length us, event | category | flops | bytes accessed | tf_op | source)
XLA Modules:
  0.0 134.5 jit_solution(9795917948837046299)
XLA Ops:
  1.5 4.6 %collective-permute-start = (bf16[30,256]{1,0:T(8,128)(2,1)S(1)}, bf16[30,256]{1,0:T(8,128)(2,1)S(1)}, u32[]{:S(2)}, u32[]{:S(2)}) collective-permute-start(bf16[30,256]{1,0:T(8,128)(2,1)S(1)} %slice.380), channel_id=1, source_target_pairs={{0,4},{4,8},{8,12},{12,16},{16,20},{20,24},{24,28},{28,32},{32,36}... | collective-permute-start | bytes 46088 | tf_op jit(solution)/shard_map/ppermute | solution.py:14
  6.8 1.9 %collective-permute-start.1 = (bf16[30,256]{1,0:T(8,128)(2,1)S(1)}, bf16[30,256]{1,0:T(8,128)(2,1)S(1)}, u32[]{:S(2)}, u32[]{:S(2)}) collective-permute-start(bf16[30,256]{1,0:T(8,128)(2,1)S(1)} %slice.381), channel_id=1, source_target_pairs={{0,4},{4,8},{8,12},{12,16},{16,20},{20,24},{24,28},{28,32},{32,36}... | collective-permute-start | bytes 46088 | tf_op jit(solution)/shard_map/ppermute | solution.py:14
  8.7 1.0 fusion.40
  9.8 1.0 fusion.41
  10.8 1.6 %collective-permute-done.1 = bf16[30,256]{1,0:T(8,128)(2,1)S(1)} collective-permute-done((bf16[30,256]{1,0:T(8,128)(2,1)S(1)}, bf16[30,256]{1,0:T(8,128)(2,1)S(1)}, u32[]{:S(2)}, u32[]{:S(2)}) %collective-permute-start.1) | collective-permute-done | bytes 15392 | tf_op jit(solution)/shard_map/ppermute | solution.py:14
  12.3 1.6 %divide_multiply_fusion = f32[1054,256]{1,0:T(8,128)S(1)} fusion(bf16[1024,256]{1,0:T(8,128)(2,1)} %param.6, bf16[30,256]{1,0:T(8,128)(2,1)S(1)} %collective-permute-done, bf16[1024,256]{1,0:T(8,128)(2,1)} %param.7, bf16[30,256]{1,0:T(8,128)(2,1)S(1)} %collective-permute-done.1), kind=kLoop, calls=%fused_computation.62 | loop fusion | flops 3237888 | bytes 2158592 | tf_op jit(solution)/shard_map/mul | solution.py:100
  13.9 5.1 %fusion.39 = (f32[1024]{0:T(1024)S(1)}, f32[1024]{0:T(1024)S(1)}, f32[1024,256]{1,0:T(8,128)}) fusion(f32[1054,256]{1,0:T(8,128)S(1)} %divide_multiply_fusion, f32[256]{0:T(256)S(1)} %bitcast.136, f32[256]{0:T(256)S(1)} %bitcast.138, f32[256]{0:T(256)S(1)} %bitcast.80, f32[256]{0:T(256)S(1)} %bitcast.82, f32[256]{0:T(256)S(1)} %bitcast.84, ...), kind=kLoop, calls=%fused_computation.126 | loop fusion | flops 16775168 | bytes 33594368 | tf_op jit(solution)/shard_map/reduce_sum | solution.py:105
  19.1 6.7 %all_to_all.47 = f32[4,1,2048]{2,1,0:T(1,128)S(1)} all-to-all(f32[4,1,2048]{2,1,0:T(1,128)S(1)} %broadcast_in_dim.12), channel_id=1, replica_groups=mesh['sp_0'=8,'sp_1'=8,'sp_2'=2,'tp'=4] {'tp'}, dimensions={0} | all-to-all | bytes 65536 | tf_op jit(solution)/shard_map/all_to_all | solution.py:19
  25.8 3.5 %multiply_reduce_fusion = (f32[256]{0:T(256)S(1)}, f32[1024]{0:T(1024)S(1)}, f32[1024]{0:T(1024)S(1)}, f32[1024,256]{1,0:T(8,128)}) fusion(f32[1024,256]{1,0:T(8,128)} %get-tuple-element.42, f32[1024]{0:T(1024)S(1)} %get-tuple-element.79, f32[1024]{0:T(1024)S(1)} %get-tuple-element.78, f32[256]{0:T(256)S(1)} %copy-done.5, ...), kind=kOutput, calls=%fused_computation.65 | convolution fusion | flops 541325056 | bytes 4737024 | tf_op jit(solution)/shard_map/dot_general | solution.py:115
  29.9 3.3 %all-to-all-start.1 = ((f32[4,1,2048]{2,1,0:T(1,128)}), f32[4,1,2048]{2,1,0:T(1,128)S(1)}, u32[]{:S(2)}, u32[]{:S(2)}) async-start(f32[4,1,2048]{2,1,0:T(1,128)} %broadcast_in_dim.13), calls=%async_computation.1 | async-start | bytes 65536 | tf_op jit(solution)/shard_map/all_to_all | solution.py:19
  33.2 4.3 %all-to-all-done.1 = f32[4,1,2048]{2,1,0:T(1,128)S(1)} async-done(((f32[4,1,2048]{2,1,0:T(1,128)}), f32[4,1,2048]{2,1,0:T(1,128)S(1)}, u32[]{:S(2)}, u32[]{:S(2)}) %all-to-all-start.1) | async-done | bytes 32800 | tf_op jit(solution)/shard_map/all_to_all | solution.py:19
  37.5 4.3 %multiply_reduce_fusion.1 = (f32[256]{0:T(256)S(1)}, f32[256]{0:T(256)S(1)}, f32[256]{0:T(256)S(1)}, f32[256]{0:T(256)S(1)}, f32[256]{0:T(256)S(1)}, /*index=5*/...) fusion(f32[1054,256]{1,0:T(8,128)S(1)} %divide_multiply_fusion,, ...), kind=kLoop, calls=%fused_computation.66 | loop fusion | flops 11267584 | bytes 22055936 | tf_op jit(solution)/shard_map/reduce_sum | solution.py:137
  41.8 1.7 %multiply_reduce_fusion.19 = (f32[256]{0:T(256)S(1)}, f32[256]{0:T(256)S(1)}, f32[256]{0:T(256)S(1)}, f32[256]{0:T(256)S(1)}, f32[256]{0:T(256)S(1)}, /*index=5*...) fusion(f32[1024,256]{1,0:T(8,128)S(1)} %get-tuple-element.41, ...), kind=kLoop, calls=%fused_computation.84 | loop fusion | flops 6812416 | bytes 14693376 | tf_op jit(solution)/shard_map/reduce_sum | solution.py:137
  43.9 7.1 %all_to_all.48 = f32[2,1,4096]{2,1,0:T(1,128)S(1)} all-to-all(f32[2,1,4096]{2,1,0:T(1,128)S(1)} %reshape.52), channel_id=1, replica_groups=mesh['sp_0'=8,'sp_1'=8,'sp_2'=2,'tp'=4] {'sp_2'}, dimensions={0} | all-to-all | bytes 65536 | tf_op jit(solution)/shard_map/all_to_all | solution.py:44
  53.0 16.3 %all-to-all-start.5 = ((f32[64,1,64]{2,1,0:T(1,128)}), f32[64,1,64]{2,1,0:T(1,128)S(1)}, u32[]{:S(2)}, u32[]{:S(2)}) async-start(f32[64,1,64]{2,1,0:T(1,128)} %bitcast.64), calls=%async_computation.5 | async-start | bytes 65536 | tf_op jit(solution)/shard_map/all_to_all | solution.py:51
  69.3 2.1 %convolution_multiply_fusion = f32[256,1024]{1,0:T(8,128)} fusion(bf16[1024,1024]{1,0:T(8,128)(2,1)S(1)} %copy-done, f32[1024,256]{1,0:T(8,128)S(1)} %copy-done.2, f32[256]{0:T(256)S(1)} %copy-done.5, f32[1024]{0:T(1024)S(1)} %get-tuple-element.79, f32[1024]{0:T(1024)S(1)} %get-tuple-element.78), kind=kOutput, calls=%fused_computation | convolution fusion | flops 539230208 | bytes 4203520 | tf_op jit(solution)/shard_map/dot_general | solution.py:161
  71.4 1.8 %reshape_reshape.7 = f32[64,2,2,1024]{3,2,1,0:T(2,128)S(1)} reshape(f32[256,1024]{1,0:T(8,128)} %convolution_multiply_fusion) | data formatting | bytes 2097152 | tf_op jit(solution)/shard_map/reshape;reshape | solution.py:39
  73.2 1.1 copy.35
  74.4 5.7 %all-to-all-done.5 = f32[64,1,64]{2,1,0:T(1,128)S(1)} async-done(((f32[64,1,64]{2,1,0:T(1,128)}), f32[64,1,64]{2,1,0:T(1,128)S(1)}, u32[]{:S(2)}, u32[]{:S(2)}) %all-to-all-start.5) | async-done | bytes 16416 | tf_op jit(solution)/shard_map/all_to_all | solution.py:51
  80.0 5.3 %all-to-all-start.2 = ((f32[2,64,2,1024]{3,2,1,0:T(2,128)}), f32[2,64,2,1024]{3,2,1,0:T(2,128)S(1)}, u32[]{:S(2)}, u32[]{:S(2)}) async-start(f32[2,64,2,1024]{3,2,1,0:T(2,128)} %bitcast.73), calls=%async_computation.2 | async-start | bytes 2097152 | tf_op jit(solution)/shard_map/all_to_all | solution.py:44
  85.5 1.7 %all-to-all-done.2 = f32[2,64,2,1024]{3,2,1,0:T(2,128)S(1)} async-done(((f32[2,64,2,1024]{3,2,1,0:T(2,128)}), f32[2,64,2,1024]{3,2,1,0:T(2,128)S(1)}, u32[]{:S(2)}, u32[]{:S(2)}) %all-to-all-start.2) | async-done | bytes 1048608 | tf_op jit(solution)/shard_map/all_to_all | solution.py:44
  87.8 5.8 %all-to-all-start.6 = ((f32[64,1,64]{2,1,0:T(1,128)}), f32[64,1,64]{2,1,0:T(1,128)S(1)}, u32[]{:S(2)}, u32[]{:S(2)}) async-start(f32[64,1,64]{2,1,0:T(1,128)} %broadcast_in_dim.15), calls=%async_computation.6 | async-start | bytes 65536 | tf_op jit(solution)/shard_map/all_to_all | solution.py:19
  93.5 1.8 %reduce_sum.384 = f32[64,2,1024]{2,1,0:T(2,128)} reduce(f32[2,64,2,1024]{3,2,1,0:T(2,128)S(1)} %all-to-all-done.2, f32[]{:T(128)} %constant.6.clone.1), dimensions={0}, to_apply=%region_6.7 | reduce | flops 131072 | bytes 1572868 | tf_op jit(solution)/shard_map/reduce_sum | solution.py:45
  95.3 3.2 %concatenate.32 = f32[1084,256]{1,0:T(8,128)S(1)} concatenate(f32[30,256]{1,0:T(8,128)S(1)} %broadcast_in_dim.14, f32[1024,256]{1,0:T(8,128)} %copy-done.1, f32[30,256]{1,0:T(8,128)S(1)} %broadcast_in_dim.14), dimensions={0} | concatenate | bytes 2220032 | tf_op jit(solution)/shard_map/concatenate | solution.py:144
  98.5 5.7 %all-to-all-done.6 = f32[64,1,64]{2,1,0:T(1,128)S(1)} async-done(((f32[64,1,64]{2,1,0:T(1,128)}), f32[64,1,64]{2,1,0:T(1,128)S(1)}, u32[]{:S(2)}, u32[]{:S(2)}) %all-to-all-start.6) | async-done | bytes 16416 | tf_op jit(solution)/shard_map/all_to_all | solution.py:19
  104.3 5.2 %all_to_all.49 = f32[2,1,4096]{2,1,0:T(1,128)S(1)} all-to-all(f32[2,1,4096]{2,1,0:T(1,128)S(1)} %reshape.54), channel_id=1, replica_groups=mesh['sp_0'=8,'sp_1'=8,'sp_2'=2,'tp'=4] {'sp_2'}, dimensions={0} | all-to-all | bytes 65536 | tf_op jit(solution)/shard_map/all_to_all | solution.py:19
  109.5 5.7 %all-to-all-start.3 = ((f32[64,2,1024]{2,1,0:T(2,128)}), f32[64,2,1024]{2,1,0:T(2,128)}, u32[]{:S(2)}, u32[]{:S(2)}) async-start(f32[64,2,1024]{2,1,0:T(2,128)} %reduce_sum.384), calls=%async_computation.3 | async-start | bytes 1048576 | tf_op jit(solution)/shard_map/all_to_all | solution.py:51
  115.2 5.4 %fusion.2 = f32[1054,256]{1,0:T(8,128)S(1)} fusion(f32[1084,256]{1,0:T(8,128)S(1)} %concatenate.32, f32[1024,256]{1,0:T(8,128)} %copy-done.1, f32[256]{0:T(256)S(1)} %bitcast.137, f32[256]{0:T(256)S(1)} %bitcast.139, f32[256]{0:T(256)S(1)} %bitcast.81, f32[256]{0:T(256)S(1)} %bitcast.83, f32[256]{0:T(256)S(1)} %bitcast.85, f32[256]{0:T(256)S(1)} %bitcast.87, ...), kind=kLoop, calls=%fused_computation.5 | loop fusion | flops 16459264 | bytes 33459200 | tf_op jit(solution)/shard_map/add | solution.py:148
  120.6 2.7 %collective-permute-start.2 = (f32[30,256]{1,0:T(8,128)S(1)}, f32[30,256]{1,0:T(8,128)S(1)}, u32[]{:S(2)}, u32[]{:S(2)}) collective-permute-start(f32[30,256]{1,0:T(8,128)S(1)} %slice.548), channel_id=1, source_target_pairs={{4,0},{8,4},{12,8},{16,12},{20,16},{24,20},{28,24},{32,28},{36,32}... | collective-permute-start | bytes 92168 | tf_op jit(solution)/shard_map/ppermute | solution.py:14
  123.4 5.4 %collective-permute-done.2 = f32[30,256]{1,0:T(8,128)S(1)} collective-permute-done((f32[30,256]{1,0:T(8,128)S(1)}, f32[30,256]{1,0:T(8,128)S(1)}, u32[]{:S(2)}, u32[]{:S(2)}) %collective-permute-start.2) | collective-permute-done | bytes 30752 | tf_op jit(solution)/shard_map/ppermute | solution.py:14
  128.7 1.4 %multiply_convert_fusion.1 = (bf16[1024,256]{1,0:T(8,128)(2,1)}, bf16[1024,256]{1,0:T(8,128)(2,1)}) fusion(bf16[1024,256]{1,0:T(8,128)(2,1)S(1)} %copy-done.3, f32[30,256]{1,0:T(8,128)S(1)} %slice_add_fusion, f32[994,256]{1,0:T(8,128)S(1)} %slice.546, bf16[1024,256]{1,0:T(8,128)(2,1)S(1)} %copy-done.4), kind=kLoop, calls=%fused_computation.98 | loop fusion | flops 3407872 | bytes 3145728 | tf_op jit(solution)/shard_map/convert_element_type | solution.py:159
  132.7 1.8 %reduce_sum.385 = f32[2,1024]{1,0:T(2,128)} reduce(f32[64,2,1024]{2,1,0:T(2,128)} %all-to-all-done.3, f32[]{:T(128)} %constant.6.clone.1), dimensions={0}, to_apply=%region_7.8 | reduce | flops 129024 | bytes 532484 | tf_op jit(solution)/shard_map/reduce_sum | solution.py:51
  (51 shorter events, 8.1 us)
Async XLA Ops:
  0.6 25.1 %copy-start = (bf16[1024,1024]{1,0:T(8,128)(2,1)S(1)}, bf16[1024,1024]{1,0:T(8,128)(2,1)}, u32[]{:S(2)}) copy-start(bf16[1024,1024]{1,0:T(8,128)(2,1)} %param.11) | copy-start | bytes 6291460
  1.5 9.2 %collective-permute-start = (bf16[30,256]{1,0:T(8,128)(2,1)S(1)}, bf16[30,256]{1,0:T(8,128)(2,1)S(1)}, u32[]{:S(2)}, u32[]{:S(2)}) collective-permute-start(bf16[30,256]{1,0:T(8,128)(2,1)S(1)} %slice.380), channel_id=1, source_target_pairs={{0,4},{4,8},{8,12},{12,16},{16,20},{20,24},{24,28},{28,32},{32,36}... | collective-permute-start | bytes 46088 | tf_op jit(solution)/shard_map/ppermute | solution.py:14
  6.8 5.5 %collective-permute-start.1 = (bf16[30,256]{1,0:T(8,128)(2,1)S(1)}, bf16[30,256]{1,0:T(8,128)(2,1)S(1)}, u32[]{:S(2)}, u32[]{:S(2)}) collective-permute-start(bf16[30,256]{1,0:T(8,128)(2,1)S(1)} %slice.381), channel_id=1, source_target_pairs={{0,4},{4,8},{8,12},{12,16},{16,20},{20,24},{24,28},{28,32},{32,36}... | collective-permute-start | bytes 46088 | tf_op jit(solution)/shard_map/ppermute | solution.py:14
  13.9 11.9 %copy-start.5 = (f32[256]{0:T(256)S(1)}, f32[256]{0:T(256)}, u32[]{:S(2)}) copy-start(f32[256]{0:T(256)} %param.9) | copy-start | bytes 3076
  29.9 7.5 %all-to-all-start.1 = ((f32[4,1,2048]{2,1,0:T(1,128)}), f32[4,1,2048]{2,1,0:T(1,128)S(1)}, u32[]{:S(2)}, u32[]{:S(2)}) async-start(f32[4,1,2048]{2,1,0:T(1,128)} %broadcast_in_dim.13), calls=%async_computation.1 | async-start | bytes 65536 | tf_op jit(solution)/shard_map/all_to_all | solution.py:19
  41.8 1.7 %copy-start.1 = (f32[1024,256]{1,0:T(8,128)}, f32[1024,256]{1,0:T(8,128)S(1)}, u32[]{:S(2)}) copy-start(f32[1024,256]{1,0:T(8,128)S(1)} %get-tuple-element.41) | copy-start | bytes 3145732
  43.5 25.7 %copy-start.2 = (f32[1024,256]{1,0:T(8,128)S(1)}, f32[1024,256]{1,0:T(8,128)}, u32[]{:S(2)}) copy-start(f32[1024,256]{1,0:T(8,128)} %get-tuple-element.42) | copy-start | bytes 3145732
  53.0 27.1 %all-to-all-start.5 = ((f32[64,1,64]{2,1,0:T(1,128)}), f32[64,1,64]{2,1,0:T(1,128)S(1)}, u32[]{:S(2)}, u32[]{:S(2)}) async-start(f32[64,1,64]{2,1,0:T(1,128)} %bitcast.64), calls=%async_computation.5 | async-start | bytes 65536 | tf_op jit(solution)/shard_map/all_to_all | solution.py:51
  80.0 7.1 %all-to-all-start.2 = ((f32[2,64,2,1024]{3,2,1,0:T(2,128)}), f32[2,64,2,1024]{3,2,1,0:T(2,128)S(1)}, u32[]{:S(2)}, u32[]{:S(2)}) async-start(f32[2,64,2,1024]{3,2,1,0:T(2,128)} %bitcast.73), calls=%async_computation.2 | async-start | bytes 2097152 | tf_op jit(solution)/shard_map/all_to_all | solution.py:44
  87.8 16.4 %all-to-all-start.6 = ((f32[64,1,64]{2,1,0:T(1,128)}), f32[64,1,64]{2,1,0:T(1,128)S(1)}, u32[]{:S(2)}, u32[]{:S(2)}) async-start(f32[64,1,64]{2,1,0:T(1,128)} %broadcast_in_dim.15), calls=%async_computation.6 | async-start | bytes 65536 | tf_op jit(solution)/shard_map/all_to_all | solution.py:19
  109.5 23.2 %all-to-all-start.3 = ((f32[64,2,1024]{2,1,0:T(2,128)}), f32[64,2,1024]{2,1,0:T(2,128)}, u32[]{:S(2)}, u32[]{:S(2)}) async-start(f32[64,2,1024]{2,1,0:T(2,128)} %reduce_sum.384), calls=%async_computation.3 | async-start | bytes 1048576 | tf_op jit(solution)/shard_map/all_to_all | solution.py:51
  120.6 8.1 %copy-start.3 = (bf16[1024,256]{1,0:T(8,128)(2,1)S(1)}, bf16[1024,256]{1,0:T(8,128)(2,1)}, u32[]{:S(2)}) copy-start(bf16[1024,256]{1,0:T(8,128)(2,1)} %param.6) | copy-start | bytes 1572868
  120.6 8.1 %copy-start.4 = (bf16[1024,256]{1,0:T(8,128)(2,1)S(1)}, bf16[1024,256]{1,0:T(8,128)(2,1)}, u32[]{:S(2)}) copy-start(bf16[1024,256]{1,0:T(8,128)(2,1)} %param.7) | copy-start | bytes 1572868
  120.6 8.1 %collective-permute-start.2 = (f32[30,256]{1,0:T(8,128)S(1)}, f32[30,256]{1,0:T(8,128)S(1)}, u32[]{:S(2)}, u32[]{:S(2)}) collective-permute-start(f32[30,256]{1,0:T(8,128)S(1)} %slice.548), channel_id=1, source_target_pairs={{4,0},{8,4},{12,8},{16,12},{20,16},{24,20},{28,24},{32,28},{36,32}... | collective-permute-start | bytes 92168 | tf_op jit(solution)/shard_map/ppermute | solution.py:14
where the time goes:
time: 137 us; the launch traced here: 134 us
  starting transfers between devices  45.5 us (33%)
  other arithmetic  25.4 us (19%)
  waiting for transfers between devices  24.4 us (18%)
  blocking collectives  18.9 us (14%)
  local copies, waits for them, and re-layouts  13.7 us (10%)
  matrix products  5.6 us (4%)
    all_to_all x2, starting transfers between devices, sum_by_axis(): return jnp.sum(lax.all_to_all(own, far, 0, 0, tiled=True), axis=0)  22 us
    all_to_all x2, blocking collectives, sent_to_all(): lax.all_to_all(jnp.broadcast_to(array[None], (peers, *array.shape)), axis...  11.9 us
    all_to_all x2, waiting for transfers between devices, sent_to_all(): lax.all_to_all(jnp.broadcast_to(array[None], (peers, *array.shape)), axis...  9.93 us
    ppermute x3, starting transfers between devices, from_behind(): return lax.ppermute(block, axis, route)  9.14 us
    all_to_all x2, starting transfers between devices, sent_to_all(): lax.all_to_all(jnp.broadcast_to(array[None], (peers, *array.shape)), axis...  9.03 us
    all_to_all x1, blocking collectives, sent_and_summed(): tiles = lax.all_to_all(in_blocks(array, dim, peers), axis, 0, 0, tiled=True)  7.08 us
    ppermute x3, waiting for transfers between devices, from_behind(): return lax.ppermute(block, axis, route)  6.91 us
    reduce_sum x2, other arithmetic, per_device(): jnp.sum(convolved_gradient * glu_out[tap:tap + row_count], axis=0)  6.03 us
  transfers between devices with their start and end apart: 8, of which 7 were waited for; matrix products, arithmetic and copies ran while one was open for 16% of the time, Pallas kernels for 0%

commit v1 on v0

v1 whole, which is shorter than its diff:
```python
import functools

import jax
import jax.numpy as jnp
from jax import lax
from jax.experimental import pallas as pl
from jax.experimental.pallas import tpu as pltpu
from jax.sharding import Mesh
from jax.sharding import PartitionSpec as P

MESH = pl.DeviceIdType.MESH
SP = ("z", "y", "c")
TP_SP = ("tp", "z", "y", "c")
F32, BF16 = jnp.float32, jnp.bfloat16
HALO = 32
LANES = 128
R = 256
RB = 32


def sigmoid(x):
    return 0.5 * jnp.tanh(0.5 * x) + 0.5


def folded(x):
    return jnp.sum(x.reshape(-1, 8, x.shape[-1]), axis=0)


def kernel(
    sizes,
    value_hbm, gate_hbm, taps_hbm, gain_hbm, w_hbm, og_hbm,
    vg_hbm, gg_hbm, proj_ref, tg_ref, ng_ref,
    value_s, gate_s, taps_s, gain_s, w_s, og_s,
    vh_s, gh_s, glu_s, sig_s, conv_s, xg_s, ag_s, act_s, act_t,
    rcol, mcol, ncol, b1, b2, cg_s, cgh_s, tacc, vg_s, gg_s,
    ex1_src, ex1_rcv, ex2_src, ex2_rcv,
    pc_src, pc_rcv, pz_src, pz_rcv, py_src, py_rcv, ps_src, ps_rcv,
    tc_src, tc_rcv, ta_src, ta_rcv1, ta_rcv2, tb_rcv1, tb_rcv2, ta_mid, ts_src, ts_rcv,
    lsem, hsem, ex1_sem, ex2_sem, cgh_sem, pc_sem, pz_sem, py_sem, ps_sem,
    tc_sem, t1a_sem, t1b_sem, t2a_sem, t2b_sem, ts_sem, osem,
):
    NZ, NY, NTP, T, C, KERNEL, CH, FACTOR = sizes
    NCH = T // R
    SUB = R // LANES
    LT = C // LANES
    z, y, c, x = (lax.axis_index(a) for a in ("z", "y", "c", "tp"))
    sp = (z * NY + y) * 2 + c
    NSP = NZ * NY * 2
    partner = {"c": 1 - c}

    def at_sp(i):
        return {"z": i // (NY * 2), "y": lax.rem(i // 2, NY), "c": lax.rem(i, 2)}

    following, preceding = at_sp(lax.rem(sp + 1, NSP)), at_sp(lax.rem(sp + NSP - 1, NSP))
    tp_peers = [lax.rem(x + d, NTP) for d in range(1, NTP)]
    y_peers = [lax.rem(y + d, NY) for d in range(1, NY)]
    z_peers = [lax.rem(z + d, NZ) for d in range(1, NZ)]

    def remote(src, dst, sems, i, device):
        return pltpu.make_async_remote_copy(
            src_ref=src, dst_ref=dst, send_sem=sems.at[(0, *i)], recv_sem=sems.at[(1, *i)],
            device_id=device, device_id_type=MESH,
        )

    barrier = pltpu.get_barrier_semaphore()
    peers = [partner, following, preceding]
    peers += [{"tp": i} for i in tp_peers] + [{"y": i} for i in y_peers] + [{"z": i} for i in z_peers]

    loads = [
        pltpu.make_async_copy(src, dst, lsem.at[i])
        for i, (src, dst) in enumerate(
            ((value_hbm, value_s), (gate_hbm, gate_s), (taps_hbm, taps_s), (gain_hbm, gain_s), (w_hbm, w_s), (og_hbm, og_s))
        )
    ]
    for copy in loads:
        copy.start()
    for device in peers:
        pl.semaphore_signal(barrier, inc=1, device_id=device, device_id_type=MESH)

    loads[0].wait()
    loads[1].wait()

    def lanes(lt):
        return slice(lt * LANES, (lt + 1) * LANES)

    def glu_block(i, _):
        rows = pl.ds(pl.multiple_of(i * RB, RB), RB)
        into = pl.ds(pl.multiple_of(HALO + i * RB, RB), RB)
        for lt in range(LT):
            s = sigmoid(gate_s[rows, lanes(lt)].astype(F32))
            sig_s[lt, rows, :] = s
            glu_s[lt, into, :] = value_s[rows, lanes(lt)].astype(F32) * s
        return 0

    lax.fori_loop(0, T // RB, glu_block, 0)

    pl.semaphore_wait(barrier, len(peers))
    halo = [
        remote(value_s.at[pl.ds(T - HALO, HALO)], vh_s, hsem, (0,), following),
        remote(gate_s.at[pl.ds(T - HALO, HALO)], gh_s, hsem, (1,), following),
    ]
    for copy in halo:
        copy.start()
    tacc[...] = jnp.zeros_like(tacc)
    loads[2].wait()
    loads[3].wait()

    def ex1(ch, d):
        return remote(ex1_src.at[ch], ex1_rcv.at[ch, x], ex1_sem, (ch, d - 1), {"tp": tp_peers[d - 1]})

    def ex2(ch, d):
        return remote(ex2_src.at[ch], ex2_rcv.at[ch, x], ex2_sem, (ch, d - 1), {"tp": tp_peers[d - 1]})

    def column_sums(blocks):
        return jnp.concatenate(blocks + [jnp.zeros((8 - len(blocks), LANES), F32)], axis=0)

    def stage1(i, _):
        ch = lax.rem(i + 1, NCH)
        first = pl.multiple_of(ch * R, R)

        @pl.when(i == NCH - 1)
        def _():
            for copy in halo:
                copy.wait_recv()
            keep = jnp.where(sp == 0, 0.0, 1.0).astype(F32)
            for lt in range(LT):
                s = sigmoid(gh_s[:, lanes(lt)].astype(F32)) * keep
                glu_s[lt, pl.ds(0, HALO), :] = vh_s[:, lanes(lt)].astype(F32) * s

        for lt in range(LT):

            def conv_block(j, _, lt=lt):
                at = pl.multiple_of(first + j * RB, RB)
                acc = taps_s[0:1, lanes(lt)] * glu_s[lt, pl.ds(at + 2, RB), :]
                for k in range(1, KERNEL):
                    acc += taps_s[k : k + 1, lanes(lt)] * glu_s[lt, pl.ds(at + 2 + k, RB), :]
                conv_s[lt, pl.ds(at, RB), :] = acc
                return 0

            lax.fori_loop(0, R // RB, conv_block, 0)
        sums, squares = [], []
        for s in range(SUB):
            rows = pl.ds(pl.multiple_of(first + s * LANES, LANES), LANES)
            total, square = 0.0, 0.0
            for lt in range(LT):
                v = conv_s[lt, rows, :]
                total, square = total + v, square + v * v
            sums.append(jnp.sum(total.T, axis=0, keepdims=True))
            squares.append(jnp.sum(square.T, axis=0, keepdims=True))
        block = column_sums(sums + squares)
        ex1_src[ch] = block
        ex1_rcv[ch, x] = block
        for d in range(1, NTP):
            ex1(ch, d).start()
        return 0

    lax.fori_loop(0, NCH, stage1, 0)

    loads[4].wait()
    loads[5].wait()

    def act_grad_block(i, _):
        rows = pl.ds(pl.multiple_of(i * R, R), R)
        g = lax.dot_general(
            og_s[rows, :], w_s[...], (((1,), (1,)), ((), ())), preferred_element_type=F32
        )
        for lt in range(LT):
            ag_s[lt, rows, :] = g[:, lanes(lt)]
        return 0

    lax.fori_loop(0, NCH, act_grad_block, 0)

    def column(row):
        return jnp.broadcast_to(row, (LANES, LANES)).T

    def stage2(i, _):
        ch = lax.rem(i + 1, NCH)
        first = pl.multiple_of(ch * R, R)
        for d in range(1, NTP):
            ex1(ch, d).wait()
        total = ex1_rcv[ch, 0]
        for t in range(1, NTP):
            total += ex1_rcv[ch, t]
        total = total * (1.0 / CH)
        mean = total[0:SUB]
        inv = lax.rsqrt(total[SUB : 2 * SUB] - mean * mean + 1e-05)
        for s in range(SUB):
            rows = pl.ds(pl.multiple_of(first + s * LANES, LANES), LANES)
            mcol[rows, :] = column(mean[s : s + 1])
            rcol[rows, :] = column(inv[s : s + 1])

        def norm_block(j, carry):
            rows = pl.ds(pl.multiple_of(first + j * RB, RB), RB)
            local = pl.ds(pl.multiple_of(j * RB, RB), RB)
            m, r = mcol[rows, :], rcol[rows, :]
            s1, s2, gains = 0.0, 0.0, []
            for lt in range(LT):
                gain = gain_s[0:1, lanes(lt)]
                xhat = (conv_s[lt, rows, :] - m) * r
                n = xhat * gain
                s = sigmoid(n)
                act_s[local, lanes(lt)] = (n * s).astype(BF16)
                ng = ag_s[lt, rows, :] * (s * (1.0 + n * (1.0 - s)))
                xg = ng * gain
                conv_s[lt, rows, :] = xhat
                xg_s[lt, rows, :] = xg
                s1, s2 = s1 + xg, s2 + xg * xhat
                gains.append(carry[lt] + folded(ng * xhat))
            b1[local, :] = s1
            b2[local, :] = s2
            return tuple(gains)

        gains = lax.fori_loop(
            0, R // RB, norm_block, tuple(jnp.zeros((8, LANES), F32) for _ in range(LT))
        )
        for lt in range(LT):
            tacc[lt, KERNEL] += gains[lt]
        blocks = [
            jnp.sum(b[s * LANES : (s + 1) * LANES, :].T, axis=0, keepdims=True)
            for b in (b1, b2)
            for s in range(SUB)
        ]
        block = column_sums(blocks)
        ex2_src[ch] = block
        ex2_rcv[ch, x] = block
        for d in range(1, NTP):
            ex2(ch, d).start()
        for lt in range(LT):
            for s in range(SUB):
                at = pl.ds(pl.multiple_of(first + s * LANES, LANES), LANES)
                act_t[lanes(lt), at] = act_s[s * LANES : (s + 1) * LANES, lanes(lt)].T
        return 0

    lax.fori_loop(0, NCH, stage2, 0)

    D = og_s.shape[1]
    H = D // 2

    def partial(owner):
        columns = pl.ds(pl.multiple_of(owner * H, H), H)
        return jnp.dot(act_t[...], og_s[:, columns], preferred_element_type=F32)

    pc_src[...] = (partial(1 - c) * FACTOR).astype(BF16)
    core_copy = remote(pc_src, pc_rcv, pc_sem, (), partner)
    core_copy.start()
    own_partial = partial(c) * FACTOR
    core_copy.wait()
    own_partial = own_partial + pc_rcv[...].astype(F32)
    ZB = C // NZ
    for i in range(NZ):
        pz_src[i] = own_partial[i * ZB : (i + 1) * ZB].astype(BF16)
    pz = [
        remote(pz_src.at[z_peers[d - 1]], pz_rcv.at[z], pz_sem, (d - 1,), {"z": z_peers[d - 1]})
        for d in range(1, NZ)
    ]
    for copy in pz:
        copy.start()
    pz_rcv[z] = pz_src[z]

    cgh = remote(cg_s.at[:, pl.ds(0, HALO), :], cgh_s, cgh_sem, (), preceding)

    def stage3(ch, _):
        first = pl.multiple_of(ch * R, R)
        for d in range(1, NTP):
            ex2(ch, d).wait()
        total = ex2_rcv[ch, 0]
        for t in range(1, NTP):
            total += ex2_rcv[ch, t]
        total = total * (1.0 / CH)
        for s in range(SUB):
            rows = pl.ds(pl.multiple_of(first + s * LANES, LANES), LANES)
            mcol[rows, :] = column(total[s : s + 1])
            ncol[rows, :] = column(total[SUB + s : SUB + s + 1])
        for lt in range(LT):

            def taps_block(j, carry, lt=lt):
                at = pl.multiple_of(first + j * RB, RB)
                rows = pl.ds(at, RB)
                g = rcol[rows, :] * (
                    xg_s[lt, rows, :] - mcol[rows, :] - conv_s[lt, rows, :] * ncol[rows, :]
                )
                cg_s[lt, rows, :] = g
                return tuple(
                    carry[k] + folded(g * glu_s[lt, pl.ds(at + 2 + k, RB), :])
                    for k in range(KERNEL)
                )

            sums = lax.fori_loop(
                0, R // RB, taps_block, tuple(jnp.zeros((8, LANES), F32) for _ in range(KERNEL))
            )
            for k in range(KERNEL):
                tacc[lt, k] += sums[k]

        @pl.when(ch == 0)
        def _():
            cgh.start()

        return 0

    lax.fori_loop(0, NCH, stage3, 0)

    for lt in range(LT):
        tc_src[lt] = jnp.sum(tacc[lt], axis=1) * FACTOR
    taps_core = remote(tc_src.at[1 - c], tc_rcv, tc_sem, (), partner)
    taps_core.start()

    def back_block(j, _):
        at = pl.multiple_of(j * RB, RB)
        rows = pl.ds(at, RB)
        for lt in range(LT):
            acc = taps_s[KERNEL - 1 : KERNEL, lanes(lt)] * cg_s[lt, rows, :]
            for k in range(1, KERNEL):
                tap = KERNEL - 1 - k
                acc += taps_s[tap : tap + 1, lanes(lt)] * cg_s[lt, pl.ds(at + k, RB), :]
            s = sig_s[lt, rows, :]
            glu = glu_s[lt, pl.ds(pl.multiple_of(at + HALO, RB), RB), :]
            vg_s[rows, lanes(lt)] = (acc * s).astype(BF16)
            gg_s[rows, lanes(lt)] = (acc * glu * (1.0 - s)).astype(BF16)
        return 0

    PER = R // RB

    def stage4(ch):
        lax.fori_loop(ch * PER, (ch + 1) * PER, back_block, 0)
        rows = pl.ds(ch * R, R)
        outs = [
            pltpu.make_async_copy(vg_s.at[rows], vg_hbm.at[rows], osem.at[ch, 0]),
            pltpu.make_async_copy(gg_s.at[rows], gg_hbm.at[rows], osem.at[ch, 1]),
        ]
        for copy in outs:
            copy.start()
        return outs

    stores = []
    stores += stage4(0)

    taps_core.wait()
    S = KERNEL + 1
    A = S // 2
    both = tc_src[c] + tc_rcv[...]
    ta_src[0] = both[0:A]
    ta_src[1] = both[A:S]
    first_hops = [
        remote(ta_src.at[0], ta_rcv1.at[y], t1a_sem, (d - 1,), {"y": y_peers[d - 1]}) for d in range(1, NY)
    ] + [
        remote(ta_src.at[1], tb_rcv1.at[z], t1b_sem, (d - 1,), {"z": z_peers[d - 1]}) for d in range(1, NZ)
    ]
    for copy in first_hops:
        copy.start()
    ta_rcv1[y] = both[0:A]
    tb_rcv1[z] = both[A:S]

    for ch in range(1, NCH - 1):
        stores += stage4(ch)
    cgh.wait()
    last = jnp.where(sp == NSP - 1, 0.0, 1.0).astype(F32)
    cg_s[:, pl.ds(T, HALO), :] = cgh_s[...] * last
    stores += stage4(NCH - 1)

    def summed(ref, n):
        total = ref[0].astype(F32)
        for i in range(1, n):
            total += ref[i].astype(F32)
        return total

    for copy in first_hops:
        copy.wait()
    half_a, half_b = summed(ta_rcv1, NY), summed(tb_rcv1, NZ)
    ta_mid[0] = half_a
    ta_mid[1] = half_b
    second_hops = [
        remote(ta_mid.at[0], ta_rcv2.at[z], t2a_sem, (d - 1,), {"z": z_peers[d - 1]}) for d in range(1, NZ)
    ] + [
        remote(ta_mid.at[1], tb_rcv2.at[y], t2b_sem, (d - 1,), {"y": y_peers[d - 1]}) for d in range(1, NY)
    ]
    for copy in second_hops:
        copy.start()
    ta_rcv2[z] = half_a
    tb_rcv2[y] = half_b

    for copy in pz:
        copy.wait()
    rows_z = summed(pz_rcv, NZ)
    YB = ZB // NY
    for i in range(NY):
        py_src[i] = rows_z[i * YB : (i + 1) * YB]
    py = [
        remote(py_src.at[y_peers[d - 1]], py_rcv.at[y], py_sem, (d - 1,), {"y": y_peers[d - 1]})
        for d in range(1, NY)
    ]
    for copy in py:
        copy.start()
    py_rcv[y] = py_src[y]

    for copy in second_hops:
        copy.wait()
    ts_src[0:A] = summed(ta_rcv2, NZ)
    ts_src[A:S] = summed(tb_rcv2, NY)
    taps_swap = remote(ts_src, ts_rcv, ts_sem, (), partner)
    taps_swap.start()

    for copy in py:
        copy.wait()
    rows_y = summed(py_rcv, NY)
    CB = YB // 2
    for i in range(2):
        ps_src[i] = rows_y[i * CB : (i + 1) * CB]
    proj_swap = remote(ps_src.at[1 - c], ps_rcv, ps_sem, (), partner)
    proj_swap.start()

    taps_swap.wait()
    mine, theirs = ts_src[...], ts_rcv[...]
    for lt in range(LT):
        v = jnp.where(c == lt, mine, theirs)
        tg_ref[:, lanes(lt)] = v[0:KERNEL]
        ng_ref[:, lanes(lt)] = v[KERNEL : KERNEL + 1]
    proj_swap.wait()
    mine, theirs = ps_src[c], ps_rcv[...]
    for i in range(2):
        proj_ref[:, i * H : (i + 1) * H] = jnp.where(c == i, mine, theirs)
    for copy in halo:
        copy.wait_send()
    for copy in stores:
        copy.wait()


def per_device(sizes, glu_value, glu_gate, conv_taps, channel_gain, proj_weight, out_grad):
    NZ, NY, NTP = sizes
    T, C = glu_value.shape
    K = conv_taps.shape[0]
    D = out_grad.shape[1]
    NCH, LT, S, A = T // R, C // LANES, K + 1, (K + 1) // 2
    ZB = C // NZ
    YB = ZB // NY
    CB = YB // 2
    H = D // 2
    factor = float(1.0 / (T * NZ * NY * 2) ** 0.5)
    params = (NZ, NY, NTP, T, C, K, C * NTP, factor)
    full = (LT, T, LANES)
    vmem, dma = pltpu.VMEM, pltpu.SemaphoreType.DMA
    any_spec = pl.BlockSpec(memory_space=pl.ANY)
    vmem_spec = pl.BlockSpec(memory_space=pltpu.VMEM)
    scratch = [
        vmem((T, C), BF16), vmem((T, C), BF16), vmem((K, C), F32), vmem((1, C), F32),
        vmem((C, D), BF16), vmem((T, D), BF16),
        vmem((HALO, C), BF16), vmem((HALO, C), BF16),
        vmem((LT, T + HALO, LANES), F32), vmem(full, F32), vmem(full, F32), vmem(full, F32), vmem(full, F32),
        vmem((R, C), BF16), vmem((C, T), BF16),
        vmem((T, LANES), F32), vmem((T, LANES), F32), vmem((T, LANES), F32),
        vmem((R, LANES), F32), vmem((R, LANES), F32),
        vmem((LT, T + HALO, LANES), F32), vmem((LT, HALO, LANES), F32),
        vmem((LT, S, 8, LANES), F32), vmem((T, C), BF16), vmem((T, C), BF16),
        vmem((NCH, 8, LANES), F32), vmem((NCH, NTP, 8, LANES), F32),
        vmem((NCH, 8, LANES), F32), vmem((NCH, NTP, 8, LANES), F32),
        vmem((C, H), BF16), vmem((C, H), BF16),
        vmem((NZ, ZB, H), BF16), vmem((NZ, ZB, H), BF16),
        vmem((NY, YB, H), F32), vmem((NY, YB, H), F32),
        vmem((2, CB, H), F32), vmem((CB, H), F32),
        vmem((LT, S, LANES), F32), vmem((S, LANES), F32),
        vmem((2, A, LANES), F32),
        vmem((NY, A, LANES), F32), vmem((NZ, A, LANES), F32),
        vmem((NZ, A, LANES), F32), vmem((NY, A, LANES), F32),
        vmem((2, A, LANES), F32), vmem((S, LANES), F32), vmem((S, LANES), F32),
        dma((6,)), dma((2, 2)), dma((2, NCH, NTP - 1)), dma((2, NCH, NTP - 1)), dma((2,)),
        dma((2,)), dma((2, NZ - 1)), dma((2, NY - 1)), dma((2,)),
        dma((2,)), dma((2, NY - 1)), dma((2, NZ - 1)), dma((2, NZ - 1)), dma((2, NY - 1)), dma((2,)),
        dma((NCH, 2)),
    ]
    value_grad, gate_grad, proj_grad, taps_grad, gain_grad = pl.pallas_call(
        functools.partial(kernel, params),
        out_shape=(
            jax.ShapeDtypeStruct((T, C), BF16),
            jax.ShapeDtypeStruct((T, C), BF16),
            jax.ShapeDtypeStruct((CB, D), F32),
            jax.ShapeDtypeStruct((K, C), F32),
            jax.ShapeDtypeStruct((1, C), F32),
        ),
        in_specs=[any_spec] * 6,
        out_specs=(any_spec, any_spec, vmem_spec, vmem_spec, vmem_spec),
        scratch_shapes=scratch,
        compiler_params=pltpu.CompilerParams(
            collective_id=0, has_side_effects=True, vmem_limit_bytes=60 * 2**20
        ),
    )(glu_value, glu_gate, conv_taps, channel_gain[None], proj_weight, out_grad)
    return value_grad, gate_grad, proj_grad, taps_grad, gain_grad[0]


def solution(mesh):
    return sized(mesh, 8, 8)


def sized(mesh, nz, ny):
    tp = mesh.shape["tp"]
    finer = Mesh(mesh.devices.reshape(nz, ny, 2, tp), ("z", "y", "c", "tp"))
    return jax.shard_map(
        functools.partial(per_device, (nz, ny, tp)),
        mesh=finer,
        in_specs=(P(SP, "tp"), P(SP, "tp"), P(None, "tp"), P("tp"), P("tp", None), P(SP, None)),
        out_specs=(P(SP, "tp"), P(SP, "tp"), P(TP_SP, None), P(None, "tp"), P("tp")),
        check_vma=False,
    )
```

time: 137 us -> 52.8 us (0.39); the launches traced: 134 us -> 52.6 us
  Pallas kernels: 0 us -> 46.4 us
  starting transfers between devices: 45.5 us -> 0 us
  other arithmetic: 25.4 us -> 0 us
  waiting for transfers between devices: 24.4 us -> 0 us
  blocking collectives: 18.9 us -> 0 us
  local copies, waits for them, and re-layouts: 13.7 us -> 5.53 us
  matrix products: 5.6 us -> 0 us
    pallas_call x0 -> x1, Pallas kernels: none -> 46.4 us  [per_device(): pl.pallas_call(functools.partial(kernel, params), out_shape=(jax.ShapeDty...]
    all_to_all x5 -> x0, starting transfers between devices: 36.3 us -> none  [the longest x2 22 us: sum_by_axis(): return jnp.sum(lax.all_to_all(own, far, 0, 0, tiled=True), axis=0)]
    all_to_all x3 -> x0, blocking collectives: 18.9 us -> none  [the longest x2 11.9 us: sent_to_all(): lax.all_to_all(jnp.broadcast_to(array[None], (peers, *array.shape)), axis...]
    all_to_all x5 -> x0, waiting for transfers between devices: 17.5 us -> none  [the longest x2 9.93 us: sent_to_all(): lax.all_to_all(jnp.broadcast_to(array[None], (peers, *array.shape)), axis...]
    reduce_sum x9 -> x0, other arithmetic: 15.5 us -> none  [the longest x2 6.03 us: per_device(): jnp.sum(convolved_gradient * glu_out[tap:tap + row_count], axis=0)]
    ppermute x3 -> x0, starting transfers between devices: 9.14 us -> none  [from_behind(): return lax.ppermute(block, axis, route)]
    ppermute x3 -> x0, waiting for transfers between devices: 6.91 us -> none  [from_behind(): return lax.ppermute(block, axis, route)]
    dot_general x2 -> x0, matrix products: 5.6 us -> none  [the longest x1 3.46 us: per_device(): lax.dot_general(out_grad, proj_weight, (((1,), (1,)), ((), ())), preferre...]
  transfers between devices with their start and end apart: 8 -> 0, of which waited for: 7 -> 0; matrix products, arithmetic and copies ran while one was open for 16% -> 0% of each run, Pallas kernels for 0% -> 0%
where the time goes in v1:
time: 52.8 us; the launch traced here: 52.6 us
  Pallas kernels  46.4 us (88%)
  local copies, waits for them, and re-layouts  5.53 us (10%)
  between operations  0.67 us (1%)
    pallas_call x1, Pallas kernels, per_device(): pl.pallas_call(functools.partial(kernel, params), out_shape=(jax.ShapeDty...  46.4 us
    unnamed x11, local copies, waits for them, and re-layouts  5.53 us

profile of v1, /device:TPU:1, one launch (start us, length us, event | category | flops | bytes accessed | tf_op | source)
XLA Modules:
  0.0 52.6 jit_solution(16642864136086945447)
XLA Ops:
  0.6 46.4 %shard_map.101 = (bf16[1024,256]{1,0:T(8,128)(2,1)}, bf16[1024,256]{1,0:T(8,128)(2,1)}, f32[2,1024]{1,0:T(2,128)}, f32[31,256]{1,0:T(8,128)}, f32[1,256]{1,0:T(1,128)}) custom-call(bf16[1024,256]{1,0:T(8,128)(2,1)} %value_hbm.1, bf16[1024,256]{1,0:T(8,128)(2,1)} %gate_hbm.1, f32[31,256]{1,0:T(8,128)} %taps_hbm.1, f32[1,256]{1,0:T(1,128)} %bitcast.3, ...), custom_call_target="tpu_custom_call" | custom-call | tf_op jit(solution)/shard_map/pallas_call | solution.py:469
  47.1 0.0 copy-start.1
  47.1 0.0 copy-start
  47.1 0.0 copy-start.2
  47.1 1.9 %copy.16 = bf16[1024,256]{1,0:T(8,128)(2,1)} copy(bf16[1024,256]{1,0:T(8,128)(2,1)} %get-tuple-element.20) | data formatting | bytes 1048576
  49.0 1.9 %copy.17 = bf16[1024,256]{1,0:T(8,128)(2,1)} copy(bf16[1024,256]{1,0:T(8,128)(2,1)} %get-tuple-element.21) | data formatting | bytes 1048576
  50.9 0.0 copy-done.1
  50.9 0.6 %copy.18 = f32[2,1024]{1,0:T(2,128)} copy(f32[2,1024]{1,0:T(2,128)S(1)} %copy-done.1) | data formatting | bytes 16384
  51.5 0.0 copy-done
  51.5 0.6 %copy.19 = f32[31,256]{1,0:T(8,128)} copy(f32[31,256]{1,0:T(8,128)S(1)} %copy-done) | data formatting | bytes 63488
  52.1 0.0 copy-done.2
  52.1 0.6 %copy.20 = f32[256]{0:T(256)} copy(f32[256]{0:T(256)S(1)} %bitcast.2) | data formatting | bytes 2048
Async XLA Ops:
  47.1 3.8 %copy-start.1 = (f32[2,1024]{1,0:T(2,128)S(1)}, f32[2,1024]{1,0:T(2,128)}, u32[]{:S(2)}) copy-start(f32[2,1024]{1,0:T(2,128)} %get-tuple-element.22) | copy-start | bytes 24580
  47.1 4.4 %copy-start = (f32[31,256]{1,0:T(8,128)S(1)}, f32[31,256]{1,0:T(8,128)}, u32[]{:S(2)}) copy-start(f32[31,256]{1,0:T(8,128)} %get-tuple-element.23) | copy-start | bytes 95236
  47.1 5.0 %copy-start.2 = (f32[1,256]{1,0:T(1,128)S(1)}, f32[1,256]{1,0:T(1,128)}, u32[]{:S(2)}) copy-start(f32[1,256]{1,0:T(1,128)} %get-tuple-element.14) | copy-start | bytes 3076

commit v2 on v1

v2 whole, which is shorter than its diff:
```python
import functools

import jax
import jax.numpy as jnp
from jax import lax
from jax.experimental import pallas as pl
from jax.experimental.pallas import tpu as pltpu
from jax.sharding import Mesh
from jax.sharding import PartitionSpec as P

MESH = pl.DeviceIdType.MESH
SP = ("z", "y", "c")
TP_SP = ("tp", "z", "y", "c")
F32, BF16 = jnp.float32, jnp.bfloat16
HALO = 32
LANES = 128
R = 256
RB = 32
GB = 64
VB = 64
NB = 32
TB = 64


def sigmoid(x):
    return 0.5 * jnp.tanh(0.5 * x) + 0.5


def folded(x):
    return jnp.sum(x.reshape(-1, 8, x.shape[-1]), axis=0)


def kernel(
    sizes,
    value_hbm, gate_hbm, taps_hbm, gain_hbm, w_hbm, og_hbm,
    vg_ref, gg_ref, proj_ref, tg_ref, ng_ref,
    value_s, gate_s, taps_s, gain_s, w_s, og_s,
    vh_s, gh_s, glu_s, sig_s, conv_s, xg_s, ag_s, act_s, act_t, act_p,
    rcol, mcol, ncol, b1, b2, cg_s, cgh_s, tacc,
    ex1_src, ex1_rcv, ex2_src, ex2_rcv,
    pc_src, pc_rcv, own_s, pa_src, pa_rcv, pb_src, pb_rcv, qa_src, qa_rcv, qb_src, qb_rcv, ps_src, ps_rcv,
    tc_src, tc_rcv, ta_src, ta_rcv1, ta_rcv2, tb_rcv1, tb_rcv2, ta_mid, ts_src, ts_rcv,
    lsem, hsem, ex1_sem, ex2_sem, cgh_sem, pc_sem, pa_sem, pb_sem, qa_sem, qb_sem, ps_sem,
    tc_sem, t1a_sem, t1b_sem, t2a_sem, t2b_sem, ts_sem,
):
    NZ, NY, NTP, T, C, KERNEL, CH, FACTOR = sizes
    NCH = T // R
    SUB = R // LANES
    LT = C // LANES
    z, y, c, x = (lax.axis_index(a) for a in ("z", "y", "c", "tp"))
    sp = (z * NY + y) * 2 + c
    NSP = NZ * NY * 2
    partner = {"c": 1 - c}

    def at_sp(i):
        return {"z": i // (NY * 2), "y": lax.rem(i // 2, NY), "c": lax.rem(i, 2)}

    following, preceding = at_sp(lax.rem(sp + 1, NSP)), at_sp(lax.rem(sp + NSP - 1, NSP))
    tp_peers = [lax.rem(x + d, NTP) for d in range(1, NTP)]
    y_peers = [lax.rem(y + d, NY) for d in range(1, NY)]
    z_peers = [lax.rem(z + d, NZ) for d in range(1, NZ)]

    def remote(src, dst, sems, i, device):
        return pltpu.make_async_remote_copy(
            src_ref=src, dst_ref=dst, send_sem=sems.at[(0, *i)], recv_sem=sems.at[(1, *i)],
            device_id=device, device_id_type=MESH,
        )

    barrier = pltpu.get_barrier_semaphore()
    peers = [partner, following, preceding]
    peers += [{"tp": i} for i in tp_peers] + [{"y": i} for i in y_peers] + [{"z": i} for i in z_peers]

    loads = [
        pltpu.make_async_copy(src, dst, lsem.at[i])
        for i, (src, dst) in enumerate(
            ((value_hbm, value_s), (gate_hbm, gate_s), (taps_hbm, taps_s), (gain_hbm, gain_s), (w_hbm, w_s), (og_hbm, og_s))
        )
    ]
    for copy in loads:
        copy.start()
    for device in peers:
        pl.semaphore_signal(barrier, inc=1, device_id=device, device_id_type=MESH)

    loads[0].wait()
    loads[1].wait()

    def lanes(lt):
        return slice(lt * LANES, (lt + 1) * LANES)

    def glu_block(i, _):
        rows = pl.ds(pl.multiple_of(i * GB, GB), GB)
        into = pl.ds(pl.multiple_of(HALO + i * GB, HALO), GB)
        for lt in range(LT):
            s = sigmoid(gate_s[rows, lanes(lt)].astype(F32))
            sig_s[lt, rows, :] = s
            glu_s[lt, into, :] = value_s[rows, lanes(lt)].astype(F32) * s
        return 0

    lax.fori_loop(0, T // GB, glu_block, 0)

    pl.semaphore_wait(barrier, len(peers))
    halo = [
        remote(value_s.at[pl.ds(T - HALO, HALO)], vh_s, hsem, (0,), following),
        remote(gate_s.at[pl.ds(T - HALO, HALO)], gh_s, hsem, (1,), following),
    ]
    for copy in halo:
        copy.start()
    tacc[...] = jnp.zeros_like(tacc)
    loads[2].wait()
    loads[3].wait()

    def ex1(ch, d):
        return remote(ex1_src.at[ch], ex1_rcv.at[ch, x], ex1_sem, (ch, d - 1), {"tp": tp_peers[d - 1]})

    def ex2(ch, d):
        return remote(ex2_src.at[ch], ex2_rcv.at[ch, x], ex2_sem, (ch, d - 1), {"tp": tp_peers[d - 1]})

    def column_sums(blocks):
        return jnp.concatenate(blocks + [jnp.zeros((8 - len(blocks), LANES), F32)], axis=0)

    def stage1(i, _):
        ch = lax.rem(i + 1, NCH)
        first = pl.multiple_of(ch * R, R)

        @pl.when(i == NCH - 1)
        def _():
            for copy in halo:
                copy.wait_recv()
            keep = jnp.where(sp == 0, 0.0, 1.0).astype(F32)
            for lt in range(LT):
                s = sigmoid(gh_s[:, lanes(lt)].astype(F32)) * keep
                glu_s[lt, pl.ds(0, HALO), :] = vh_s[:, lanes(lt)].astype(F32) * s

        for lt in range(LT):

            def conv_block(j, _, lt=lt):
                at = pl.multiple_of(first + j * VB, VB)
                acc = taps_s[0:1, lanes(lt)] * glu_s[lt, pl.ds(at + 2, VB), :]
                for k in range(1, KERNEL):
                    acc += taps_s[k : k + 1, lanes(lt)] * glu_s[lt, pl.ds(at + 2 + k, VB), :]
                conv_s[lt, pl.ds(at, VB), :] = acc
                return 0

            lax.fori_loop(0, R // VB, conv_block, 0)
        sums, squares = [], []
        for s in range(SUB):
            rows = pl.ds(pl.multiple_of(first + s * LANES, LANES), LANES)
            total, square = 0.0, 0.0
            for lt in range(LT):
                v = conv_s[lt, rows, :]
                total, square = total + v, square + v * v
            sums.append(jnp.sum(total.T, axis=0, keepdims=True))
            squares.append(jnp.sum(square.T, axis=0, keepdims=True))
        block = column_sums(sums + squares)
        ex1_src[ch] = block
        ex1_rcv[ch, x] = block
        for d in range(1, NTP):
            ex1(ch, d).start()
        return 0

    lax.fori_loop(0, NCH, stage1, 0)

    loads[4].wait()
    loads[5].wait()

    def act_grad_block(i, _):
        rows = pl.ds(pl.multiple_of(i * R, R), R)
        g = lax.dot_general(
            og_s[rows, :], w_s[...], (((1,), (1,)), ((), ())), preferred_element_type=F32
        )
        for lt in range(LT):
            ag_s[lt, rows, :] = g[:, lanes(lt)]
        return 0

    lax.fori_loop(0, NCH, act_grad_block, 0)

    def column(row):
        return jnp.broadcast_to(row, (LANES, LANES)).T

    def stage2(i, _):
        ch = lax.rem(i + 1, NCH)
        first = pl.multiple_of(ch * R, R)
        for d in range(1, NTP):
            ex1(ch, d).wait()
        total = ex1_rcv[ch, 0]
        for t in range(1, NTP):
            total += ex1_rcv[ch, t]
        total = total * (1.0 / CH)
        mean = total[0:SUB]
        inv = lax.rsqrt(total[SUB : 2 * SUB] - mean * mean + 1e-05)
        for s in range(SUB):
            rows = pl.ds(pl.multiple_of(first + s * LANES, LANES), LANES)
            mcol[rows, :] = column(mean[s : s + 1])
            rcol[rows, :] = column(inv[s : s + 1])

        def norm_block(j, carry):
            rows = pl.ds(pl.multiple_of(first + j * NB, NB), NB)
            local = pl.ds(pl.multiple_of(j * NB, NB), NB)
            m, r = mcol[rows, :], rcol[rows, :]
            s1, s2, gains = 0.0, 0.0, []
            for lt in range(LT):
                gain = gain_s[0:1, lanes(lt)]
                xhat = (conv_s[lt, rows, :] - m) * r
                n = xhat * gain
                s = sigmoid(n)
                act_s[local, lanes(lt)] = (n * s).astype(BF16)
                ng = ag_s[lt, rows, :] * (s * (1.0 + n * (1.0 - s)))
                xg = ng * gain
                conv_s[lt, rows, :] = xhat
                xg_s[lt, rows, :] = xg
                s1, s2 = s1 + xg, s2 + xg * xhat
                gains.append(carry[lt] + folded(ng * xhat))
            b1[local, :] = s1
            b2[local, :] = s2
            return tuple(gains)

        gains = lax.fori_loop(
            0, R // NB, norm_block, tuple(jnp.zeros((8, LANES), F32) for _ in range(LT))
        )
        for lt in range(LT):
            tacc[lt, KERNEL] += gains[lt]
        blocks = [
            jnp.sum(b[s * LANES : (s + 1) * LANES, :].T, axis=0, keepdims=True)
            for b in (b1, b2)
            for s in range(SUB)
        ]
        block = column_sums(blocks)
        ex2_src[ch] = block
        ex2_rcv[ch, x] = block
        for d in range(1, NTP):
            ex2(ch, d).start()
        for lt in range(LT):
            for s in range(SUB):
                at = pl.ds(pl.multiple_of(first + s * LANES, LANES), LANES)
                act_t[lanes(lt), at] = act_s[s * LANES : (s + 1) * LANES, lanes(lt)].T
        return 0

    lax.fori_loop(0, NCH - 1, stage2, 0)

    cgh = remote(cg_s.at[:, pl.ds(0, HALO), :], cgh_s, cgh_sem, (), preceding)

    def stage3(ch):
        first = ch * R
        for d in range(1, NTP):
            ex2(ch, d).wait()
        total = ex2_rcv[ch, 0]
        for t in range(1, NTP):
            total += ex2_rcv[ch, t]
        total = total * (1.0 / CH)
        for s in range(SUB):
            rows = pl.ds(first + s * LANES, LANES)
            mcol[rows, :] = column(total[s : s + 1])
            ncol[rows, :] = column(total[SUB + s : SUB + s + 1])
        for lt in range(LT):

            def taps_block(j, carry, lt=lt):
                at = pl.multiple_of(first + j * TB, TB)
                rows = pl.ds(at, TB)
                g = rcol[rows, :] * (
                    xg_s[lt, rows, :] - mcol[rows, :] - conv_s[lt, rows, :] * ncol[rows, :]
                )
                cg_s[lt, rows, :] = g
                return tuple(
                    carry[k] + folded(g * glu_s[lt, pl.ds(at + 2 + k, TB), :])
                    for k in range(KERNEL)
                )

            sums = lax.fori_loop(
                0, R // TB, taps_block, tuple(jnp.zeros((8, LANES), F32) for _ in range(KERNEL))
            )
            for k in range(KERNEL):
                tacc[lt, k] += sums[k]

    def back_block(j, _):
        at = pl.multiple_of(j * RB, RB)
        rows = pl.ds(at, RB)
        for lt in range(LT):
            acc = taps_s[KERNEL - 1 : KERNEL, lanes(lt)] * cg_s[lt, rows, :]
            for k in range(1, KERNEL):
                tap = KERNEL - 1 - k
                acc += taps_s[tap : tap + 1, lanes(lt)] * cg_s[lt, pl.ds(at + k, RB), :]
            s = sig_s[lt, rows, :]
            glu = glu_s[lt, pl.ds(pl.multiple_of(at + HALO, RB), RB), :]
            vg_ref[rows, lanes(lt)] = (acc * s).astype(BF16)
            gg_ref[rows, lanes(lt)] = (acc * glu * (1.0 - s)).astype(BF16)
        return 0

    PER = R // RB

    def stage4(ch):
        lax.fori_loop(ch * PER, (ch + 1) * PER, back_block, 0)

    def summed(ref, n):
        total = ref[0].astype(F32)
        for i in range(1, n):
            total += ref[i].astype(F32)
        return total

    order = [(i + 1) % NCH for i in range(NCH)]
    stage3(order[0])
    stage2(NCH - 1, 0)

    D = og_s.shape[1]
    H = D // 2
    Q = H // 2
    B = C // (NZ * NY)
    shape = (C, C)
    i = lax.broadcasted_iota(jnp.int32, shape, 0)
    j = lax.broadcasted_iota(jnp.int32, shape, 1)
    source = ((i // B) % NZ) * (NY * B) + (i // (B * NZ)) * B + i % B
    permutation = jnp.where(j == source, 1.0, 0.0).astype(BF16)
    act_p[...] = jnp.dot(permutation, act_t[...], preferred_element_type=F32).astype(BF16)

    def partial(owner, part):
        columns = pl.ds(pl.multiple_of(owner * H + part * Q, Q), Q)
        rows = (act_t, act_p)[part]
        return jnp.dot(rows[...], og_s[:, columns], preferred_element_type=F32) * FACTOR

    for part in range(2):
        pc_src[part] = partial(1 - c, part).astype(BF16)
    core_copy = remote(pc_src, pc_rcv, pc_sem, (), partner)
    core_copy.start()
    for part in range(2):
        own_s[part] = partial(c, part)

    stage3(order[1])

    core_copy.wait()
    ZB, YB = C // NZ, C // NY
    own = own_s[0] + pc_rcv[0].astype(F32)
    for i in range(NZ):
        pa_src[i] = own[i * ZB : (i + 1) * ZB].astype(BF16)
    own = own_s[1] + pc_rcv[1].astype(F32)
    for i in range(NY):
        pb_src[i] = own[i * YB : (i + 1) * YB].astype(BF16)

    def to_z(src, dst, sems):
        return [
            remote(src.at[z_peers[d - 1]], dst.at[z], sems, (d - 1,), {"z": z_peers[d - 1]}) for d in range(1, NZ)
        ]

    def to_y(src, dst, sems):
        return [
            remote(src.at[y_peers[d - 1]], dst.at[y], sems, (d - 1,), {"y": y_peers[d - 1]}) for d in range(1, NY)
        ]

    proj_first = to_z(pa_src, pa_rcv, pa_sem) + to_y(pb_src, pb_rcv, pb_sem)
    for copy in proj_first:
        copy.start()
    pa_rcv[z] = pa_src[z]
    pb_rcv[y] = pb_src[y]

    for ch in order[2:-1]:
        stage3(ch)
    stage4(order[0])
    stage3(0)
    cgh.start()

    S = KERNEL + 1
    A = S // 2
    for lt in range(LT):
        tc_src[:, lanes(lt)] = jnp.sum(tacc[lt], axis=1) * FACTOR
    taps_core = remote(tc_src, tc_rcv, tc_sem, (), partner)
    taps_first = [
        remote(ta_src.at[0], ta_rcv1.at[y], t1a_sem, (d - 1,), {"y": y_peers[d - 1]}) for d in range(1, NY)
    ] + [
        remote(ta_src.at[1], tb_rcv1.at[z], t1b_sem, (d - 1,), {"z": z_peers[d - 1]}) for d in range(1, NZ)
    ]
    taps_second = [
        remote(ta_mid.at[0], ta_rcv2.at[z], t2a_sem, (d - 1,), {"z": z_peers[d - 1]}) for d in range(1, NZ)
    ] + [
        remote(ta_mid.at[1], tb_rcv2.at[y], t2b_sem, (d - 1,), {"y": y_peers[d - 1]}) for d in range(1, NY)
    ]
    taps_swap = remote(ts_src, ts_rcv, ts_sem, (), partner)

    @pl.when(c == 0)
    def _():
        taps_core.start()

    stage4(0)

    @pl.when(c == 1)
    def _():
        taps_core.wait_recv()
        both = tc_src[...] + tc_rcv[...]
        ta_src[0] = both[0:A]
        ta_src[1] = both[A:S]
        for copy in taps_first:
            copy.start()
        ta_rcv1[y] = both[0:A]
        tb_rcv1[z] = both[A:S]

    for ch in order[1:-2]:
        stage4(ch)
    cgh.wait()
    last = jnp.where(sp == NSP - 1, 0.0, 1.0).astype(F32)
    cg_s[:, pl.ds(T, HALO), :] = cgh_s[...] * last
    stage4(NCH - 1)

    for copy in proj_first:
        copy.wait()
    part_a, part_b = summed(pa_rcv, NZ), summed(pb_rcv, NY)
    for i in range(NY):
        qa_src[i] = part_a[i * B : (i + 1) * B]
    for i in range(NZ):
        qb_src[i] = part_b[i * B : (i + 1) * B]
    proj_second = to_y(qa_src, qa_rcv, qa_sem) + to_z(qb_src, qb_rcv, qb_sem)
    for copy in proj_second:
        copy.start()
    qa_rcv[y] = qa_src[y]
    qb_rcv[z] = qb_src[z]

    @pl.when(c == 1)
    def _():
        for copy in taps_first:
            copy.wait()
        half_a, half_b = summed(ta_rcv1, NY), summed(tb_rcv1, NZ)
        ta_mid[0] = half_a
        ta_mid[1] = half_b
        for copy in taps_second:
            copy.start()
        ta_rcv2[z] = half_a
        tb_rcv2[y] = half_b

    for copy in proj_second:
        copy.wait()
    done_a, done_b = summed(qa_rcv, NY), summed(qb_rcv, NZ)
    CB = B // 2
    for i in range(2):
        ps_src[i, :, 0:Q] = done_a[i * CB : (i + 1) * CB]
        ps_src[i, :, Q:H] = done_b[i * CB : (i + 1) * CB]
    proj_swap = remote(ps_src.at[1 - c], ps_rcv, ps_sem, (), partner)
    proj_swap.start()

    @pl.when(c == 1)
    def _():
        for copy in taps_second:
            copy.wait()
        ts_src[0:A] = summed(ta_rcv2, NZ)
        ts_src[A:S] = summed(tb_rcv2, NY)
        taps_swap.start()
        tg_ref[...] = ts_src[0:KERNEL]
        ng_ref[...] = ts_src[KERNEL : KERNEL + 1]

    proj_swap.wait()
    mine, theirs = ps_src[c], ps_rcv[...]
    for i in range(2):
        proj_ref[:, i * H : (i + 1) * H] = jnp.where(c == i, mine, theirs)
    for copy in halo:
        copy.wait_send()

    @pl.when(c == 1)
    def _():
        taps_swap.wait_send()

    @pl.when(c == 0)
    def _():
        taps_core.wait_send()
        taps_swap.wait_recv()
        tg_ref[...] = ts_rcv[0:KERNEL]
        ng_ref[...] = ts_rcv[KERNEL : KERNEL + 1]


def store_kernel(*refs):
    n = len(refs) // 2
    sems = refs[-1]
    copies = [pltpu.make_async_copy(refs[i], refs[n + i], sems.at[i]) for i in range(n)]
    for copy in copies:
        copy.start()
    for copy in copies:
        copy.wait()


def per_device(sizes, glu_value, glu_gate, conv_taps, channel_gain, proj_weight, out_grad):
    NZ, NY, NTP = sizes
    T, C = glu_value.shape
    K = conv_taps.shape[0]
    D = out_grad.shape[1]
    NCH, LT, S, A = T // R, C // LANES, K + 1, (K + 1) // 2
    ZB, YB, B = C // NZ, C // NY, C // (NZ * NY)
    CB = B // 2
    H, Q = D // 2, D // 4
    factor = float(1.0 / (T * NZ * NY * 2) ** 0.5)
    params = (NZ, NY, NTP, T, C, K, C * NTP, factor)
    full = (LT, T, LANES)
    vmem, dma = pltpu.VMEM, pltpu.SemaphoreType.DMA
    any_spec = pl.BlockSpec(memory_space=pltpu.HBM)
    vmem_spec = pl.BlockSpec(memory_space=pltpu.VMEM)
    scratch = [
        vmem((T, C), BF16), vmem((T, C), BF16), vmem((K, C), F32), vmem((1, C), F32),
        vmem((C, D), BF16), vmem((T, D), BF16),
        vmem((HALO, C), BF16), vmem((HALO, C), BF16),
        vmem((LT, T + HALO, LANES), F32), vmem(full, F32), vmem(full, F32), vmem(full, F32), vmem(full, F32),
        vmem((R, C), BF16), vmem((C, T), BF16), vmem((C, T), BF16),
        vmem((T, LANES), F32), vmem((T, LANES), F32), vmem((T, LANES), F32),
        vmem((R, LANES), F32), vmem((R, LANES), F32),
        vmem((LT, T + HALO, LANES), F32), vmem((LT, HALO, LANES), F32),
        vmem((LT, S, 8, LANES), F32),
        vmem((NCH, 8, LANES), F32), vmem((NCH, NTP, 8, LANES), F32),
        vmem((NCH, 8, LANES), F32), vmem((NCH, NTP, 8, LANES), F32),
        vmem((2, C, Q), BF16), vmem((2, C, Q), BF16), vmem((2, C, Q), F32),
        vmem((NZ, ZB, Q), BF16), vmem((NZ, ZB, Q), BF16),
        vmem((NY, YB, Q), BF16), vmem((NY, YB, Q), BF16),
        vmem((NY, B, Q), F32), vmem((NY, B, Q), F32),
        vmem((NZ, B, Q), F32), vmem((NZ, B, Q), F32),
        vmem((2, CB, H), F32), vmem((CB, H), F32),
        vmem((S, C), F32), vmem((S, C), F32),
        vmem((2, A, C), F32),
        vmem((NY, A, C), F32), vmem((NZ, A, C), F32),
        vmem((NZ, A, C), F32), vmem((NY, A, C), F32),
        vmem((2, A, C), F32), vmem((S, C), F32), vmem((S, C), F32),
        dma((6,)), dma((2, 2)), dma((2, NCH, NTP - 1)), dma((2, NCH, NTP - 1)), dma((2,)),
        dma((2,)), dma((2, NZ - 1)), dma((2, NY - 1)), dma((2, NY - 1)), dma((2, NZ - 1)), dma((2,)),
        dma((2,)), dma((2, NY - 1)), dma((2, NZ - 1)), dma((2, NZ - 1)), dma((2, NY - 1)), dma((2,)),
    ]
    results = (
        jax.ShapeDtypeStruct((T, C), BF16),
        jax.ShapeDtypeStruct((T, C), BF16),
        jax.ShapeDtypeStruct((CB, D), F32),
        jax.ShapeDtypeStruct((K, C), F32),
        jax.ShapeDtypeStruct((1, C), F32),
    )
    held = pl.pallas_call(
        functools.partial(kernel, params),
        out_shape=results,
        in_specs=[any_spec] * 6,
        out_specs=(vmem_spec,) * 5,
        scratch_shapes=scratch,
        compiler_params=pltpu.CompilerParams(
            collective_id=0, has_side_effects=True, vmem_limit_bytes=40 * 2**20
        ),
    )(*(
        pltpu.with_memory_space_constraint(a, pltpu.HBM)
        for a in (glu_value, glu_gate, conv_taps, channel_gain[None], proj_weight, out_grad)
    ))
    value_grad, gate_grad, proj_grad, taps_grad, gain_grad = pl.pallas_call(
        store_kernel,
        out_shape=results,
        in_specs=[vmem_spec] * 5,
        out_specs=(any_spec,) * 5,
        scratch_shapes=[dma((5,))],
        compiler_params=pltpu.CompilerParams(vmem_limit_bytes=8 * 2**20),
    )(*held)
    return value_grad, gate_grad, proj_grad, taps_grad, gain_grad[0]


def solution(mesh):
    return sized(mesh, 8, 8)


def sized(mesh, nz, ny):
    tp = mesh.shape["tp"]
    finer = Mesh(mesh.devices.reshape(nz, ny, 2, tp), ("z", "y", "c", "tp"))
    return jax.shard_map(
        functools.partial(per_device, (nz, ny, tp)),
        mesh=finer,
        in_specs=(P(SP, "tp"), P(SP, "tp"), P(None, "tp"), P("tp"), P("tp", None), P(SP, None)),
        out_specs=(P(SP, "tp"), P(SP, "tp"), P(TP_SP, None), P(None, "tp"), P("tp")),
        check_vma=False,
    )
```

time: 52.8 us -> 46.1 us (0.87)
  local copies, waits for them, and re-layouts: 5.53 us -> 0 us
  Pallas kernels: 46.4 us -> 45.3 us
    unnamed x11 -> x0, local copies, waits for them, and re-layouts: 5.53 us -> none
    pallas_call x1 -> x2, Pallas kernels: 46.4 us -> 45.3 us  [the longest x1 44.3 us: per_device(): pl.pallas_call(functools.partial(kernel, params), out_shape=results, in_s...]
where the time goes in v2:
time: 46.1 us; the launch traced here: 45.9 us
  Pallas kernels  45.3 us (98%)
  between operations  0.64 us (1%)
    pallas_call x1, Pallas kernels, per_device(): pl.pallas_call(functools.partial(kernel, params), out_shape=results, in_s...  44.3 us
    pallas_call x1, Pallas kernels, per_device(): pl.pallas_call(store_kernel, out_shape=results, in_specs=[vmem_spec] * 5,...  1.02 us

profile of v2, /device:TPU:1, one launch (start us, length us, event | category | flops | bytes accessed | tf_op | source)
XLA Modules:
  0.0 45.9 jit_solution(14809280196043232508)
XLA Ops:
  0.6 44.3 %shard_map.101 = (bf16[1024,256]{1,0:T(8,128)(2,1)S(1)}, bf16[1024,256]{1,0:T(8,128)(2,1)S(1)}, f32[2,1024]{1,0:T(2,128)S(1)}, f32[31,256]{1,0:T(8,128)S(1)}, f32[1,256]{1,0:T(1,128)S(1)}) custom-call(bf16[1024,256]{1,0:T(8,128)(2,1)} %value_hbm.1, bf16[1024,256]{1,0:T(8,128)(2,1)} %gate_hbm.1, f32[31,256]{1,0:T(8,128)} %taps_hbm.1, f32[1,256]{1,0:T(1,128)} %bitcast.2, ...), custom_call_target="tpu_custom_call" | custom-call | tf_op jit(solution)/shard_map/pallas_call | solution.py:523
  44.9 1.0 %shard_map.102 = (bf16[1024,256]{1,0:T(8,128)(2,1)}, bf16[1024,256]{1,0:T(8,128)(2,1)}, f32[2,1024]{1,0:T(2,128)}, f32[31,256]{1,0:T(8,128)}, f32[1,256]{1,0:T(1,128)}) custom-call(bf16[1024,256]{1,0:T(8,128)(2,1)S(1)} %get-tuple-element.15.refs_0_, bf16[1024,256]{1,0:T(8,128)(2,1)S(1)} %get-tuple-element.16.refs_1_, ...), custom_call_target="tpu_custom_call" | custom-call | tf_op jit(solution)/shard_map/pallas_call | solution.py:536

commit v3 on v2

v3 whole, which is shorter than its diff:
```python
import functools

import jax
import jax.numpy as jnp
from jax import lax
from jax.experimental import pallas as pl
from jax.experimental.pallas import tpu as pltpu
from jax.sharding import Mesh
from jax.sharding import PartitionSpec as P

MESH = pl.DeviceIdType.MESH
SP = ("z", "y", "c")
TP_SP = ("tp", "z", "y", "c")
F32, BF16 = jnp.float32, jnp.bfloat16
HALO = 32
LANES = 128
R = 256
RB = 32
GB = 64
VB = 64
NB = 32
TB = 64
AB = 512


def sigmoid(x):
    return 0.5 * jnp.tanh(0.5 * x) + 0.5


def folded(x):
    return jnp.sum(x.reshape(-1, 8, x.shape[-1]), axis=0)


def kernel(
    sizes,
    value_hbm, gate_hbm, taps_hbm, gain_hbm, w_hbm, og_hbm,
    vg_ref, gg_ref, proj_ref, tg_ref, ng_ref,
    value_s, gate_s, taps_s, gain_s, w_s, og_s,
    hv_s, glu_s, sig_s, conv_s, xg_s, ag_s, act_s, act_t, act_p,
    rcol, mcol, ncol, b1, b2, cg_s, cgh_s, tacc,
    ex1_src, ex1_rcv, ex2_src, ex2_rcv,
    pc_src, pc_rcv, own_s, p1_src, p1_rcv, p2_src, p2_rcv, ps_src, ps_rcv,
    tc_src, tc_rcv, t1_src, t1_rcv, t2_src, t2_rcv, ts_src, ts_rcv,
    lsem, hsem, ex1_sem, ex2_sem, cgh_sem, pc_sem, p1_sem, p2_sem, ps_sem, tc_sem, t1_sem, t2_sem, ts_sem,
):
    NZ, NY, NTP, T, C, KERNEL, CH, FACTOR = sizes
    NBLK = T // LANES
    BIG = (T - 2 * LANES) // R
    chunks = [(LANES + i * R, R) for i in range(BIG)] + [(T - LANES, LANES), (0, LANES)]
    LT = C // LANES
    z, y, c, x = (lax.axis_index(a) for a in ("z", "y", "c", "tp"))
    sp = (z * NY + y) * 2 + c
    NSP = NZ * NY * 2
    partner = {"c": 1 - c}

    def at_sp(i):
        return {"z": i // (NY * 2), "y": lax.rem(i // 2, NY), "c": lax.rem(i, 2)}

    following, preceding = at_sp(lax.rem(sp + 1, NSP)), at_sp(lax.rem(sp + NSP - 1, NSP))
    tp_peers = [lax.rem(x + d, NTP) for d in range(1, NTP)]
    y_peers = [lax.rem(y + d, NY) for d in range(1, NY)]
    z_peers = [lax.rem(z + d, NZ) for d in range(1, NZ)]

    def remote(src, dst, sems, device, i=0):
        return pltpu.make_async_remote_copy(
            src_ref=src, dst_ref=dst, send_sem=sems.at[0], recv_sem=sems.at[1 + i],
            device_id=device, device_id_type=MESH,
        )

    barrier = pltpu.get_barrier_semaphore()
    peers = [partner, following, preceding]
    peers += [{"tp": i} for i in tp_peers] + [{"y": i} for i in y_peers] + [{"z": i} for i in z_peers]

    loads = [
        pltpu.make_async_copy(src, dst, lsem.at[i])
        for i, (src, dst) in enumerate(
            ((value_hbm, value_s), (gate_hbm, gate_s), (taps_hbm, taps_s), (gain_hbm, gain_s), (w_hbm, w_s), (og_hbm, og_s))
        )
    ]
    for copy in loads:
        copy.start()
    for device in peers:
        pl.semaphore_signal(barrier, inc=1, device_id=device, device_id_type=MESH)

    loads[0].wait()
    loads[1].wait()

    def lanes(lt):
        return slice(lt * LANES, (lt + 1) * LANES)

    def glu_block(i, _):
        rows = pl.ds(pl.multiple_of(i * GB, GB), GB)
        into = pl.ds(pl.multiple_of(HALO + i * GB, HALO), GB)
        for lt in range(LT):
            s = sigmoid(gate_s[rows, lanes(lt)].astype(F32))
            sig_s[lt, rows, :] = s
            glu_s[lt, into, :] = value_s[rows, lanes(lt)].astype(F32) * s
        return 0

    lax.fori_loop(0, T // GB, glu_block, 0)

    pl.semaphore_wait(barrier, len(peers))
    tail = pl.ds(T - HALO, HALO)
    remote(value_s.at[tail], hv_s.at[0], hsem, following).start()
    remote(gate_s.at[tail], hv_s.at[1], hsem, following).start()
    halo = remote(hv_s, hv_s, hsem, following)
    tacc[...] = jnp.zeros_like(tacc)
    loads[2].wait()
    loads[3].wait()

    def exchange(src, rcv, sem, n):
        first, size = chunks[n]
        blocks = pl.ds(first // LANES, size // LANES)
        for peer in tp_peers:
            remote(src.at[blocks], rcv.at[x, blocks], sem, {"tp": peer}, n).start()

    def received(rcv, sem, block, count, n):
        sample = rcv.at[pl.ds(0, NTP - 1), pl.ds(block, count)]
        remote(sample, sample, sem, partner, n).wait_recv()

    def record(src, rcv, block, rows):
        for i, row in enumerate(rows):
            src[block, i : i + 1, :] = row
            rcv[x, block, i : i + 1, :] = row

    def row_sums(v):
        return jnp.sum(v.T, axis=0, keepdims=True)

    def conv_stats(block):
        rows = pl.ds(pl.multiple_of(block * LANES, LANES), LANES)
        total, square = 0.0, 0.0
        for lt in range(LT):
            v = conv_s[lt, rows, :]
            total, square = total + v, square + v * v
        return row_sums(total), row_sums(square)

    def conv_block(block):
        for lt in range(LT):
            for half in range(LANES // VB):
                at = pl.multiple_of(block * LANES + half * VB, VB)
                acc = taps_s[0:1, lanes(lt)] * glu_s[lt, pl.ds(at + 2, VB), :]
                for k in range(1, KERNEL):
                    acc += taps_s[k : k + 1, lanes(lt)] * glu_s[lt, pl.ds(at + 2 + k, VB), :]
                conv_s[lt, pl.ds(at, VB), :] = acc

    conv_block(1)

    def stage1(block, _):
        sums = conv_stats(block)

        conv_block(lax.rem(block + 1, NBLK))
        record(ex1_src, ex1_rcv, block, sums)
        for n, (first, size) in enumerate(chunks[:-1]):

            @pl.when(block == (first + size) // LANES - 1)
            def _(n=n):
                exchange(ex1_src, ex1_rcv, ex1_sem, n)

        @pl.when(block == NBLK - 2)
        def _():
            halo.wait_recv()
            keep = jnp.where(sp == 0, 0.0, 1.0).astype(F32)
            for lt in range(LT):
                s = sigmoid(hv_s[1, :, lanes(lt)].astype(F32)) * keep
                glu_s[lt, pl.ds(0, HALO), :] = hv_s[0, :, lanes(lt)].astype(F32) * s

        return 0

    lax.fori_loop(1, NBLK, stage1, 0)
    record(ex1_src, ex1_rcv, 0, conv_stats(0))
    exchange(ex1_src, ex1_rcv, ex1_sem, len(chunks) - 1)

    loads[4].wait()
    loads[5].wait()

    def act_grad_block(i, _):
        rows = pl.ds(pl.multiple_of(i * AB, AB), AB)
        g = lax.dot_general(
            og_s[rows, :], w_s[...], (((1,), (1,)), ((), ())), preferred_element_type=F32
        )
        for lt in range(LT):
            ag_s[lt, rows, :] = g[:, lanes(lt)]
        return 0

    lax.fori_loop(0, T // AB, act_grad_block, 0)

    def column(row):
        return jnp.broadcast_to(row, (LANES, LANES)).T

    def totals(rcv, sem, block, count, n):
        received(rcv, sem, block, count, n)
        both = []
        for s in range(count):
            total = rcv[0, block + s]
            for t in range(1, NTP):
                total += rcv[t, block + s]
            both.append(total * (1.0 / CH))
        return both

    def stage2(n, first, size):
        block, count = first // LANES, size // LANES
        for s, total in enumerate(totals(ex1_rcv, ex1_sem, block, count, n)):
            mean = total[0:1]
            inv = lax.rsqrt(total[1:2] - mean * mean + 1e-05)
            rows = pl.ds(pl.multiple_of(first + s * LANES, LANES), LANES)
            mcol[rows, :] = column(mean)
            rcol[rows, :] = column(inv)

        def norm_block(j, carry):
            rows = pl.ds(pl.multiple_of(first + j * NB, NB), NB)
            local = pl.ds(pl.multiple_of(j * NB, NB), NB)
            m, r = mcol[rows, :], rcol[rows, :]
            s1, s2, gains = 0.0, 0.0, []
            for lt in range(LT):
                gain = gain_s[0:1, lanes(lt)]
                xhat = (conv_s[lt, rows, :] - m) * r
                n = xhat * gain
                s = sigmoid(n)
                act_s[local, lanes(lt)] = (n * s).astype(BF16)
                ng = ag_s[lt, rows, :] * (s * (1.0 + n * (1.0 - s)))
                xg = ng * gain
                conv_s[lt, rows, :] = xhat
                xg_s[lt, rows, :] = xg
                s1, s2 = s1 + xg, s2 + xg * xhat
                gains.append(carry[lt] + folded(ng * xhat))
            b1[local, :] = s1
            b2[local, :] = s2
            return tuple(gains)

        gains = lax.fori_loop(
            0, size // NB, norm_block, tuple(jnp.zeros((8, LANES), F32) for _ in range(LT))
        )
        for lt in range(LT):
            tacc[lt, KERNEL] += gains[lt]
        for s in range(count):
            part = slice(s * LANES, (s + 1) * LANES)
            record(ex2_src, ex2_rcv, block + s, (row_sums(b1[part, :]), row_sums(b2[part, :])))
        for peer in tp_peers:
            blocks = pl.ds(block, count)
            remote(ex2_src.at[blocks], ex2_rcv.at[x, blocks], ex2_sem, {"tp": peer}, n).start()
        for lt in range(LT):
            for s in range(count):
                at = pl.ds(pl.multiple_of(first + s * LANES, LANES), LANES)
                act_t[lanes(lt), at] = act_s[s * LANES : (s + 1) * LANES, lanes(lt)].T

    def stage2_big(i, _):
        stage2(i, pl.multiple_of(LANES + i * R, LANES), R)
        return 0

    lax.fori_loop(0, BIG, stage2_big, 0)
    stage2(BIG, *chunks[BIG])
    stage2(BIG + 1, *chunks[BIG + 1])

    cgh = remote(cg_s.at[:, pl.ds(0, HALO), :], cgh_s, cgh_sem, preceding)

    def stage3(n):
        first, size = chunks[n]
        block, count = first // LANES, size // LANES
        for s, total in enumerate(totals(ex2_rcv, ex2_sem, block, count, n)):
            rows = pl.ds(first + s * LANES, LANES)
            mcol[rows, :] = column(total[0:1])
            ncol[rows, :] = column(total[1:2])
        for lt in range(LT):

            def taps_block(j, carry, lt=lt):
                at = pl.multiple_of(first + j * TB, TB)
                rows = pl.ds(at, TB)
                g = rcol[rows, :] * (
                    xg_s[lt, rows, :] - mcol[rows, :] - conv_s[lt, rows, :] * ncol[rows, :]
                )
                cg_s[lt, rows, :] = g
                return tuple(
                    carry[k] + folded(g * glu_s[lt, pl.ds(at + 2 + k, TB), :])
                    for k in range(KERNEL)
                )

            sums = lax.fori_loop(
                0, size // TB, taps_block, tuple(jnp.zeros((8, LANES), F32) for _ in range(KERNEL))
            )
            for k in range(KERNEL):
                tacc[lt, k] += sums[k]

    def back_block(j, _):
        at = pl.multiple_of(j * RB, RB)
        rows = pl.ds(at, RB)
        for lt in range(LT):
            acc = taps_s[KERNEL - 1 : KERNEL, lanes(lt)] * cg_s[lt, rows, :]
            for k in range(1, KERNEL):
                tap = KERNEL - 1 - k
                acc += taps_s[tap : tap + 1, lanes(lt)] * cg_s[lt, pl.ds(at + k, RB), :]
            s = sig_s[lt, rows, :]
            glu = glu_s[lt, pl.ds(pl.multiple_of(at + HALO, RB), RB), :]
            vg_ref[rows, lanes(lt)] = (acc * s).astype(BF16)
            gg_ref[rows, lanes(lt)] = (acc * glu * (1.0 - s)).astype(BF16)
        return 0

    def stage4(first, last):
        lax.fori_loop(first // RB, last // RB, back_block, 0)

    def summed(ref, n):
        total = ref[0].astype(F32)
        for i in range(1, n):
            total += ref[i].astype(F32)
        return total

    D = og_s.shape[1]
    H = D // 2
    Q = H // 2
    B = C // (NZ * NY)
    shape = (C, C)
    i = lax.broadcasted_iota(jnp.int32, shape, 0)
    j = lax.broadcasted_iota(jnp.int32, shape, 1)
    source = ((i // B) % NZ) * (NY * B) + (i // (B * NZ)) * B + i % B
    permutation = jnp.where(j == source, 1.0, 0.0).astype(BF16)
    act_p[...] = jnp.dot(permutation, act_t[...], preferred_element_type=F32).astype(BF16)

    def partial(owner, part):
        columns = pl.ds(pl.multiple_of(owner * H + part * Q, Q), Q)
        rows = (act_t, act_p)[part]
        return jnp.dot(rows[...], og_s[:, columns], preferred_element_type=F32) * FACTOR

    for part in range(2):
        pc_src[part] = partial(1 - c, part).astype(BF16)
    core_copy = remote(pc_src, pc_rcv, pc_sem, partner)
    core_copy.start()
    for part in range(2):
        own_s[part] = partial(c, part)

    stage3(0)

    core_copy.wait()
    N = NZ
    ZB = C // N

    def both_ways(src, dst, sems, swapped):
        z_part, y_part = (1, 0) if swapped else (0, 1)
        for i in z_peers:
            remote(src(z_part, i), dst.at[z_part, z], sems, {"z": i}).start()
        for i in y_peers:
            remote(src(y_part, i), dst.at[y_part, y], sems, {"y": i}).start()

    def finish(dst, sems):
        sample = dst.at[:, pl.ds(0, N - 1)]
        remote(sample, sample, sems, partner).wait()

    for part in range(2):
        own = own_s[part] + pc_rcv[part].astype(F32)
        for i in range(N):
            p1_src[part, i] = own[i * ZB : (i + 1) * ZB].astype(BF16)
    both_ways(lambda part, i: p1_src.at[part, i], p1_rcv, p1_sem, False)
    p1_rcv[0, z] = p1_src[0, z]
    p1_rcv[1, y] = p1_src[1, y]

    for n in range(1, len(chunks)):
        stage3(n)
    cgh.start()

    S = KERNEL + 1
    A = S // 2
    for lt in range(LT):
        tc_src[:, lanes(lt)] = jnp.sum(tacc[lt], axis=1) * FACTOR
    taps_core = remote(tc_src, tc_rcv, tc_sem, partner)
    taps_swap = remote(ts_src, ts_rcv, ts_sem, partner)

    @pl.when(c == 0)
    def _():
        taps_core.start()

    stage4(0, R)

    @pl.when(c == 1)
    def _():
        taps_core.wait_recv()
        both = tc_src[...] + tc_rcv[...]
        t1_src[0] = both[0:A]
        t1_src[1] = both[A:S]
        both_ways(lambda part, i: t1_src.at[part], t1_rcv, t1_sem, False)
        t1_rcv[0, z] = both[0:A]
        t1_rcv[1, y] = both[A:S]

    stage4(R, T - R)
    cgh.wait()
    last = jnp.where(sp == NSP - 1, 0.0, 1.0).astype(F32)
    cg_s[:, pl.ds(T, HALO), :] = cgh_s[...] * last
    stage4(T - R, T)

    finish(p1_rcv, p1_sem)
    for part in range(2):
        sums = summed(p1_rcv.at[part], N)
        for i in range(N):
            p2_src[part, i] = sums[i * B : (i + 1) * B]
    both_ways(lambda part, i: p2_src.at[part, i], p2_rcv, p2_sem, True)
    p2_rcv[0, y] = p2_src[0, y]
    p2_rcv[1, z] = p2_src[1, z]

    @pl.when(c == 1)
    def _():
        finish(t1_rcv, t1_sem)
        half_a, half_b = summed(t1_rcv.at[0], N), summed(t1_rcv.at[1], N)
        t2_src[0] = half_a
        t2_src[1] = half_b
        both_ways(lambda part, i: t2_src.at[part], t2_rcv, t2_sem, True)
        t2_rcv[0, y] = half_a
        t2_rcv[1, z] = half_b

    finish(p2_rcv, p2_sem)
    done_a, done_b = summed(p2_rcv.at[0], N), summed(p2_rcv.at[1], N)
    CB = B // 2
    for i in range(2):
        ps_src[i, :, 0:Q] = done_a[i * CB : (i + 1) * CB]
        ps_src[i, :, Q:H] = done_b[i * CB : (i + 1) * CB]
    proj_swap = remote(ps_src.at[1 - c], ps_rcv, ps_sem, partner)
    proj_swap.start()

    @pl.when(c == 1)
    def _():
        finish(t2_rcv, t2_sem)
        ts_src[0:A] = summed(t2_rcv.at[0], N)
        ts_src[A:S] = summed(t2_rcv.at[1], N)
        taps_swap.start()
        tg_ref[...] = ts_src[0:KERNEL]
        ng_ref[...] = ts_src[KERNEL : KERNEL + 1]

    proj_swap.wait()
    mine, theirs = ps_src[c], ps_rcv[...]
    for i in range(2):
        proj_ref[:, i * H : (i + 1) * H] = jnp.where(c == i, mine, theirs)
    halo.wait_send()
    for rcv, sem in ((ex1_rcv, ex1_sem), (ex2_rcv, ex2_sem)):
        sample = rcv.at[pl.ds(0, NTP - 1)]
        remote(sample, sample, sem, partner).wait_send()

    @pl.when(c == 1)
    def _():
        taps_swap.wait_send()

    @pl.when(c == 0)
    def _():
        taps_core.wait_send()
        taps_swap.wait_recv()
        tg_ref[...] = ts_rcv[0:KERNEL]
        ng_ref[...] = ts_rcv[KERNEL : KERNEL + 1]


def store_kernel(*refs):
    n = len(refs) // 2
    sems = refs[-1]
    copies = [pltpu.make_async_copy(refs[i], refs[n + i], sems.at[i]) for i in range(n)]
    for copy in copies:
        copy.start()
    for copy in copies:
        copy.wait()


def per_device(sizes, glu_value, glu_gate, conv_taps, channel_gain, proj_weight, out_grad):
    NZ, NY, NTP = sizes
    T, C = glu_value.shape
    K = conv_taps.shape[0]
    D = out_grad.shape[1]
    LT, S, A = C // LANES, K + 1, (K + 1) // 2
    N, ZB, B = NZ, C // NZ, C // (NZ * NY)
    NBLK = T // LANES
    NCH = (T - 2 * LANES) // R + 2
    CB = B // 2
    H, Q = D // 2, D // 4
    factor = float(1.0 / (T * NZ * NY * 2) ** 0.5)
    params = (NZ, NY, NTP, T, C, K, C * NTP, factor)
    full = (LT, T, LANES)
    vmem, dma = pltpu.VMEM, pltpu.SemaphoreType.DMA
    any_spec = pl.BlockSpec(memory_space=pltpu.HBM)
    vmem_spec = pl.BlockSpec(memory_space=pltpu.VMEM)
    scratch = [
        vmem((T, C), BF16), vmem((T, C), BF16), vmem((K, C), F32), vmem((1, C), F32),
        vmem((C, D), BF16), vmem((T, D), BF16),
        vmem((2, HALO, C), BF16),
        vmem((LT, T + HALO, LANES), F32), vmem(full, F32), vmem(full, F32), vmem(full, F32), vmem(full, F32),
        vmem((R, C), BF16), vmem((C, T), BF16), vmem((C, T), BF16),
        vmem((T, LANES), F32), vmem((T, LANES), F32), vmem((T, LANES), F32),
        vmem((R, LANES), F32), vmem((R, LANES), F32),
        vmem((LT, T + HALO, LANES), F32), vmem((LT, HALO, LANES), F32),
        vmem((LT, S, 8, LANES), F32),
        vmem((NBLK, 2, LANES), F32), vmem((NTP, NBLK, 2, LANES), F32),
        vmem((NBLK, 2, LANES), F32), vmem((NTP, NBLK, 2, LANES), F32),
        vmem((2, C, Q), BF16), vmem((2, C, Q), BF16), vmem((2, C, Q), F32),
        vmem((2, N, ZB, Q), BF16), vmem((2, N, ZB, Q), BF16),
        vmem((2, N, B, Q), F32), vmem((2, N, B, Q), F32),
        vmem((2, CB, H), F32), vmem((CB, H), F32),
        vmem((S, C), F32), vmem((S, C), F32),
        vmem((2, A, C), F32), vmem((2, N, A, C), F32),
        vmem((2, A, C), F32), vmem((2, N, A, C), F32),
        vmem((S, C), F32), vmem((S, C), F32),
        dma((6,)), dma((2,)), dma((1 + NCH,)), dma((1 + NCH,)), dma((2,)),
    ] + [dma((2,))] * 8 + [
    ]
    results = (
        jax.ShapeDtypeStruct((T, C), BF16),
        jax.ShapeDtypeStruct((T, C), BF16),
        jax.ShapeDtypeStruct((CB, D), F32),
        jax.ShapeDtypeStruct((K, C), F32),
        jax.ShapeDtypeStruct((1, C), F32),
    )
    held = pl.pallas_call(
        functools.partial(kernel, params),
        out_shape=results,
        in_specs=[any_spec] * 6,
        out_specs=(vmem_spec,) * 5,
        scratch_shapes=scratch,
        compiler_params=pltpu.CompilerParams(
            collective_id=0, has_side_effects=True, vmem_limit_bytes=40 * 2**20
        ),
    )(*(
        pltpu.with_memory_space_constraint(a, pltpu.HBM)
        for a in (glu_value, glu_gate, conv_taps, channel_gain[None], proj_weight, out_grad)
    ))
    value_grad, gate_grad, proj_grad, taps_grad, gain_grad = pl.pallas_call(
        store_kernel,
        out_shape=results,
        in_specs=[vmem_spec] * 5,
        out_specs=(any_spec,) * 5,
        scratch_shapes=[dma((5,))],
        compiler_params=pltpu.CompilerParams(vmem_limit_bytes=8 * 2**20),
    )(*held)
    return value_grad, gate_grad, proj_grad, taps_grad, gain_grad[0]


def solution(mesh):
    return sized(mesh, 8, 8)


def sized(mesh, nz, ny):
    tp = mesh.shape["tp"]
    finer = Mesh(mesh.devices.reshape(nz, ny, 2, tp), ("z", "y", "c", "tp"))
    return jax.shard_map(
        functools.partial(per_device, (nz, ny, tp)),
        mesh=finer,
        in_specs=(P(SP, "tp"), P(SP, "tp"), P(None, "tp"), P("tp"), P("tp", None), P(SP, None)),
        out_specs=(P(SP, "tp"), P(SP, "tp"), P(TP_SP, None), P(None, "tp"), P("tp")),
        check_vma=False,
    )
```

time: 46.1 us -> 41.4 us (0.90)
  Pallas kernels: 45.3 us -> 40.7 us
    pallas_call x1, Pallas kernels: 44.3 us -> 39.6 us  [per_device(): pl.pallas_call(functools.partial(kernel, params), out_shape=results, in_s...]
where the time goes in v3:
time: 41.4 us; the launch traced here: 41.3 us
  Pallas kernels  40.7 us (98%)
  between operations  0.64 us (2%)
    pallas_call x1, Pallas kernels, per_device(): pl.pallas_call(functools.partial(kernel, params), out_shape=results, in_s...  39.6 us
    pallas_call x1, Pallas kernels, per_device(): pl.pallas_call(store_kernel, out_shape=results, in_specs=[vmem_spec] * 5,...  1.02 us

profile of v3, /device:TPU:1, one launch (start us, length us, event | category | flops | bytes accessed | tf_op | source)
XLA Modules:
  0.0 41.3 jit_solution(8463881115388346110)
XLA Ops:
  0.6 39.6 %shard_map.101 = (bf16[1024,256]{1,0:T(8,128)(2,1)S(1)}, bf16[1024,256]{1,0:T(8,128)(2,1)S(1)}, f32[2,1024]{1,0:T(2,128)S(1)}, f32[31,256]{1,0:T(8,128)S(1)}, f32[1,256]{1,0:T(1,128)S(1)}) custom-call(bf16[1024,256]{1,0:T(8,128)(2,1)} %value_hbm.1, bf16[1024,256]{1,0:T(8,128)(2,1)} %gate_hbm.1, f32[31,256]{1,0:T(8,128)} %taps_hbm.1, f32[1,256]{1,0:T(1,128)} %bitcast.2, ...), custom_call_target="tpu_custom_call" | custom-call | tf_op jit(solution)/shard_map/pallas_call | solution.py:502
  40.3 1.0 %shard_map.102 = (bf16[1024,256]{1,0:T(8,128)(2,1)}, bf16[1024,256]{1,0:T(8,128)(2,1)}, f32[2,1024]{1,0:T(2,128)}, f32[31,256]{1,0:T(8,128)}, f32[1,256]{1,0:T(1,128)}) custom-call(bf16[1024,256]{1,0:T(8,128)(2,1)S(1)} %get-tuple-element.15.refs_0_, bf16[1024,256]{1,0:T(8,128)(2,1)S(1)} %get-tuple-element.16.refs_1_, ...), custom_call_target="tpu_custom_call" | custom-call | tf_op jit(solution)/shard_map/pallas_call | solution.py:515

commit v4 on v3

--- a/solution.py
+++ b/solution.py
@@ -36,8 +36,8 @@
     value_hbm, gate_hbm, taps_hbm, gain_hbm, w_hbm, og_hbm,
     vg_ref, gg_ref, proj_ref, tg_ref, ng_ref,
     value_s, gate_s, taps_s, gain_s, w_s, og_s,
-    hv_s, glu_s, sig_s, conv_s, xg_s, ag_s, act_s, act_t, act_p,
-    rcol, mcol, ncol, b1, b2, cg_s, cgh_s, tacc,
+    hv_s, glu_s, sig_s, conv_s, xg_s, ag_s, act_t, act_p,
+    rcol, mcol, ncol, cg_s, cgh_s, tacc,
     ex1_src, ex1_rcv, ex2_src, ex2_rcv,
     pc_src, pc_rcv, own_s, p1_src, p1_rcv, p2_src, p2_rcv, ps_src, ps_rcv,
     tc_src, tc_rcv, t1_src, t1_rcv, t2_src, t2_rcv, ts_src, ts_rcv,
@@ -57,9 +57,11 @@
         return {"z": i // (NY * 2), "y": lax.rem(i // 2, NY), "c": lax.rem(i, 2)}
 
     following, preceding = at_sp(lax.rem(sp + 1, NSP)), at_sp(lax.rem(sp + NSP - 1, NSP))
-    tp_peers = [lax.rem(x + d, NTP) for d in range(1, NTP)]
-    y_peers = [lax.rem(y + d, NY) for d in range(1, NY)]
-    z_peers = [lax.rem(z + d, NZ) for d in range(1, NZ)]
+
+    def others(i, n):
+        return [lax.rem(i + d, n) for d in sorted(range(1, n), key=lambda d: -min(d, n - d))]
+
+    tp_peers, y_peers, z_peers = others(x, NTP), others(y, NY), others(z, NZ)
 
     def remote(src, dst, sems, device, i=0):
         return pltpu.make_async_remote_copy(
@@ -126,6 +128,13 @@
     def row_sums(v):
         return jnp.sum(v.T, axis=0, keepdims=True)
 
+    def windows(ref, lt, at, size):
+        for s in range(8):
+            steps = len(range(s, KERNEL, 8))
+            wide = ref[lt, pl.ds(at + s, size + 8 * (steps - 1)), :]
+            for m in range(steps):
+                yield s + 8 * m, wide[8 * m : 8 * m + size]
+
     def conv_stats(block):
         rows = pl.ds(pl.multiple_of(block * LANES, LANES), LANES)
         total, square = 0.0, 0.0
@@ -138,9 +147,9 @@
         for lt in range(LT):
             for half in range(LANES // VB):
                 at = pl.multiple_of(block * LANES + half * VB, VB)
-                acc = taps_s[0:1, lanes(lt)] * glu_s[lt, pl.ds(at + 2, VB), :]
-                for k in range(1, KERNEL):
-                    acc += taps_s[k : k + 1, lanes(lt)] * glu_s[lt, pl.ds(at + 2 + k, VB), :]
+                acc = jnp.zeros((VB, LANES), F32)
+                for k, window in windows(glu_s, lt, at + 2, VB):
+                    acc += taps_s[k : k + 1, lanes(lt)] * window
                 conv_s[lt, pl.ds(at, VB), :] = acc
 
     conv_block(1)
@@ -199,49 +208,44 @@
 
     def stage2(n, first, size):
         block, count = first // LANES, size // LANES
+        activ = []
         for s, total in enumerate(totals(ex1_rcv, ex1_sem, block, count, n)):
             mean = total[0:1]
             inv = lax.rsqrt(total[1:2] - mean * mean + 1e-05)
-            rows = pl.ds(pl.multiple_of(first + s * LANES, LANES), LANES)
-            mcol[rows, :] = column(mean)
-            rcol[rows, :] = column(inv)
-
-        def norm_block(j, carry):
-            rows = pl.ds(pl.multiple_of(first + j * NB, NB), NB)
-            local = pl.ds(pl.multiple_of(j * NB, NB), NB)
-            m, r = mcol[rows, :], rcol[rows, :]
-            s1, s2, gains = 0.0, 0.0, []
+            m, r = column(mean), column(inv)
+            start = first + s * LANES
+            rcol[pl.ds(pl.multiple_of(start, LANES), LANES), :] = r
+            sums1, sums2, acts = [], [], [[] for _ in range(LT)]
+            gains = [0.0] * LT
+            for j in range(0, LANES, NB):
+                rows = pl.ds(pl.multiple_of(start + j, NB), NB)
+                s1, s2 = 0.0, 0.0
+                for lt in range(LT):
+                    gain = gain_s[0:1, lanes(lt)]
+                    xhat = (conv_s[lt, rows, :] - m[j : j + NB]) * r[j : j + NB]
+                    n_ = xhat * gain
+                    g = sigmoid(n_)
+                    acts[lt].append((n_ * g).astype(BF16))
+                    ng = ag_s[lt, rows, :] * (g * (1.0 + n_ * (1.0 - g)))
+                    xg = ng * gain
+                    conv_s[lt, rows, :] = xhat
+                    xg_s[lt, rows, :] = xg
+                    s1, s2 = s1 + xg, s2 + xg * xhat
+                    gains[lt] += folded(ng * xhat)
+                sums1.append(s1)
+                sums2.append(s2)
             for lt in range(LT):
-                gain = gain_s[0:1, lanes(lt)]
-                xhat = (conv_s[lt, rows, :] - m) * r
-                n = xhat * gain
-                s = sigmoid(n)
-                act_s[local, lanes(lt)] = (n * s).astype(BF16)
-                ng = ag_s[lt, rows, :] * (s * (1.0 + n * (1.0 - s)))
-                xg = ng * gain
-                conv_s[lt, rows, :] = xhat
-                xg_s[lt, rows, :] = xg
-                s1, s2 = s1 + xg, s2 + xg * xhat
-                gains.append(carry[lt] + folded(ng * xhat))
-            b1[local, :] = s1
-            b2[local, :] = s2
-            return tuple(gains)
-
-        gains = lax.fori_loop(
-            0, size // NB, norm_block, tuple(jnp.zeros((8, LANES), F32) for _ in range(LT))
-        )
-        for lt in range(LT):
-            tacc[lt, KERNEL] += gains[lt]
-        for s in range(count):
-            part = slice(s * LANES, (s + 1) * LANES)
-            record(ex2_src, ex2_rcv, block + s, (row_sums(b1[part, :]), row_sums(b2[part, :])))
+                tacc[lt, KERNEL] += gains[lt]
+            rows = (row_sums(jnp.concatenate(v, axis=0)) for v in (sums1, sums2))
+            record(ex2_src, ex2_rcv, block + s, rows)
+            activ.append([jnp.concatenate(v, axis=0) for v in acts])
         for peer in tp_peers:
             blocks = pl.ds(block, count)
             remote(ex2_src.at[blocks], ex2_rcv.at[x, blocks], ex2_sem, {"tp": peer}, n).start()
-        for lt in range(LT):
-            for s in range(count):
+        for s in range(count):
+            for lt in range(LT):
                 at = pl.ds(pl.multiple_of(first + s * LANES, LANES), LANES)
-                act_t[lanes(lt), at] = act_s[s * LANES : (s + 1) * LANES, lanes(lt)].T
+                act_t[lanes(lt), at] = activ[s][lt].T
 
     def stage2_big(i, _):
         stage2(i, pl.multiple_of(LANES + i * R, LANES), R)
@@ -269,10 +273,10 @@
                     xg_s[lt, rows, :] - mcol[rows, :] - conv_s[lt, rows, :] * ncol[rows, :]
                 )
                 cg_s[lt, rows, :] = g
-                return tuple(
-                    carry[k] + folded(g * glu_s[lt, pl.ds(at + 2 + k, TB), :])
-                    for k in range(KERNEL)
-                )
+                carry = list(carry)
+                for k, window in windows(glu_s, lt, at + 2, TB):
+                    carry[k] += folded(g * window)
+                return tuple(carry)
 
             sums = lax.fori_loop(
                 0, size // TB, taps_block, tuple(jnp.zeros((8, LANES), F32) for _ in range(KERNEL))
@@ -284,10 +288,10 @@
         at = pl.multiple_of(j * RB, RB)
         rows = pl.ds(at, RB)
         for lt in range(LT):
-            acc = taps_s[KERNEL - 1 : KERNEL, lanes(lt)] * cg_s[lt, rows, :]
-            for k in range(1, KERNEL):
+            acc = jnp.zeros((RB, LANES), F32)
+            for k, window in windows(cg_s, lt, at, RB):
                 tap = KERNEL - 1 - k
-                acc += taps_s[tap : tap + 1, lanes(lt)] * cg_s[lt, pl.ds(at + k, RB), :]
+                acc += taps_s[tap : tap + 1, lanes(lt)] * window
             s = sig_s[lt, rows, :]
             glu = glu_s[lt, pl.ds(pl.multiple_of(at + HALO, RB), RB), :]
             vg_ref[rows, lanes(lt)] = (acc * s).astype(BF16)
@@ -474,9 +478,8 @@
         vmem((C, D), BF16), vmem((T, D), BF16),
         vmem((2, HALO, C), BF16),
         vmem((LT, T + HALO, LANES), F32), vmem(full, F32), vmem(full, F32), vmem(full, F32), vmem(full, F32),
-        vmem((R, C), BF16), vmem((C, T), BF16), vmem((C, T), BF16),
+        vmem((C, T), BF16), vmem((C, T), BF16),
         vmem((T, LANES), F32), vmem((T, LANES), F32), vmem((T, LANES), F32),
-        vmem((R, LANES), F32), vmem((R, LANES), F32),
         vmem((LT, T + HALO, LANES), F32), vmem((LT, HALO, LANES), F32),
         vmem((LT, S, 8, LANES), F32),
         vmem((NBLK, 2, LANES), F32), vmem((NTP, NBLK, 2, LANES), F32),

time: 41.4 us -> 39.6 us (0.957)
  Pallas kernels: 40.7 us -> 38.9 us
    pallas_call x1, Pallas kernels: 39.6 us -> 37.9 us  [per_device(): pl.pallas_call(functools.partial(kernel, params), out_shape=results, in_s...]
where the time goes in v4:
time: 39.6 us; the launch traced here: 39.5 us
  Pallas kernels  38.9 us (98%)
  between operations  0.64 us (2%)
    pallas_call x1, Pallas kernels, per_device(): pl.pallas_call(functools.partial(kernel, params), out_shape=results, in_s...  37.9 us
    pallas_call x1, Pallas kernels, per_device(): pl.pallas_call(store_kernel, out_shape=results, in_specs=[vmem_spec] * 5,...  1.02 us

profile of v4, /device:TPU:1, one launch (start us, length us, event | category | flops | bytes accessed | tf_op | source)
XLA Modules:
  0.0 39.5 jit_solution(17183431786584527296)
XLA Ops:
  0.6 37.9 %shard_map.101 = (bf16[1024,256]{1,0:T(8,128)(2,1)S(1)}, bf16[1024,256]{1,0:T(8,128)(2,1)S(1)}, f32[2,1024]{1,0:T(2,128)S(1)}, f32[31,256]{1,0:T(8,128)S(1)}, f32[1,256]{1,0:T(1,128)S(1)}) custom-call(bf16[1024,256]{1,0:T(8,128)(2,1)} %value_hbm.1, bf16[1024,256]{1,0:T(8,128)(2,1)} %gate_hbm.1, f32[31,256]{1,0:T(8,128)} %taps_hbm.1, f32[1,256]{1,0:T(1,128)} %bitcast.2, ...), custom_call_target="tpu_custom_call" | custom-call | tf_op jit(solution)/shard_map/pallas_call | solution.py:505
  38.5 1.0 %shard_map.102 = (bf16[1024,256]{1,0:T(8,128)(2,1)}, bf16[1024,256]{1,0:T(8,128)(2,1)}, f32[2,1024]{1,0:T(2,128)}, f32[31,256]{1,0:T(8,128)}, f32[1,256]{1,0:T(1,128)}) custom-call(bf16[1024,256]{1,0:T(8,128)(2,1)S(1)} %get-tuple-element.15.refs_0_, bf16[1024,256]{1,0:T(8,128)(2,1)S(1)} %get-tuple-element.16.refs_1_, ...), custom_call_target="tpu_custom_call" | custom-call | tf_op jit(solution)/shard_map/pallas_call | solution.py:518

commit v5 on v4

--- a/solution.py
+++ b/solution.py
@@ -41,7 +41,7 @@
     ex1_src, ex1_rcv, ex2_src, ex2_rcv,
     pc_src, pc_rcv, own_s, p1_src, p1_rcv, p2_src, p2_rcv, ps_src, ps_rcv,
     tc_src, tc_rcv, t1_src, t1_rcv, t2_src, t2_rcv, ts_src, ts_rcv,
-    lsem, hsem, ex1_sem, ex2_sem, cgh_sem, pc_sem, p1_sem, p2_sem, ps_sem, tc_sem, t1_sem, t2_sem, ts_sem,
+    lsem, hsem, ex1_sem, ex2_sem, cgh_sem, pc_sem, p1_sem, p2_sem, ps_sem, tc_sem, t1_sem, t2_sem, ts_sem, rounds,
 ):
     NZ, NY, NTP, T, C, KERNEL, CH, FACTOR = sizes
     NBLK = T // LANES
@@ -70,8 +70,20 @@
         )
 
     barrier = pltpu.get_barrier_semaphore()
-    peers = [partner, following, preceding]
-    peers += [{"tp": i} for i in tp_peers] + [{"y": i} for i in y_peers] + [{"z": i} for i in z_peers]
+    near = [{"y": lax.rem(y + d, NY)} for d in (1, NY - 1)] + [{"z": lax.rem(z + d, NZ)} for d in (1, NZ - 1)]
+    peers = [partner, following, preceding] + [{"tp": i} for i in tp_peers] + near
+
+    ROUNDS = NY // 2 - 1
+
+    def tell(r):
+        for device in near:
+            pl.semaphore_signal(rounds.at[r], inc=1, device_id=device, device_id_type=MESH)
+
+    def hear(r):
+        pl.semaphore_wait(rounds.at[r], len(near))
+        if r + 1 < ROUNDS:
+            tell(r + 1)
+
 
     loads = [
         pltpu.make_async_copy(src, dst, lsem.at[i])
@@ -102,6 +114,7 @@
     lax.fori_loop(0, T // GB, glu_block, 0)
 
     pl.semaphore_wait(barrier, len(peers))
+    tell(0)
     tail = pl.ds(T - HALO, HALO)
     remote(value_s.at[tail], hv_s.at[0], hsem, following).start()
     remote(gate_s.at[tail], hv_s.at[1], hsem, following).start()
@@ -179,6 +192,7 @@
     record(ex1_src, ex1_rcv, 0, conv_stats(0))
     exchange(ex1_src, ex1_rcv, ex1_sem, len(chunks) - 1)
 
+    hear(0)
     loads[4].wait()
     loads[5].wait()
 
@@ -192,6 +206,8 @@
         return 0
 
     lax.fori_loop(0, T // AB, act_grad_block, 0)
+
+    hear(1)
 
     def column(row):
         return jnp.broadcast_to(row, (LANES, LANES)).T
@@ -327,6 +343,7 @@
         pc_src[part] = partial(1 - c, part).astype(BF16)
     core_copy = remote(pc_src, pc_rcv, pc_sem, partner)
     core_copy.start()
+    hear(2)
     for part in range(2):
         own_s[part] = partial(c, part)
 
@@ -493,8 +510,7 @@
         vmem((2, A, C), F32), vmem((2, N, A, C), F32),
         vmem((S, C), F32), vmem((S, C), F32),
         dma((6,)), dma((2,)), dma((1 + NCH,)), dma((1 + NCH,)), dma((2,)),
-    ] + [dma((2,))] * 8 + [
-    ]
+    ] + [dma((2,))] * 8 + [pltpu.SemaphoreType.REGULAR((max(NY // 2 - 1, 1),))]
     results = (
         jax.ShapeDtypeStruct((T, C), BF16),
         jax.ShapeDtypeStruct((T, C), BF16),

time: 39.6 us -> 38.8 us (0.980)
  Pallas kernels: 38.9 us -> 38.1 us
    pallas_call x1, Pallas kernels: 37.9 us -> 37.1 us  [per_device(): pl.pallas_call(functools.partial(kernel, params), out_shape=results, in_s...]
where the time goes in v5:
time: 38.8 us; the launch traced here: 38.7 us
  Pallas kernels  38.1 us (98%)
  between operations  0.64 us (2%)
    pallas_call x1, Pallas kernels, per_device(): pl.pallas_call(functools.partial(kernel, params), out_shape=results, in_s...  37.1 us
    pallas_call x1, Pallas kernels, per_device(): pl.pallas_call(store_kernel, out_shape=results, in_specs=[vmem_spec] * 5,...  1.02 us

profile of v5, /device:TPU:1, one launch (start us, length us, event | category | flops | bytes accessed | tf_op | source)
XLA Modules:
  0.0 38.7 jit_solution(1302500923879557443)
XLA Ops:
  0.6 37.1 %shard_map.101 = (bf16[1024,256]{1,0:T(8,128)(2,1)S(1)}, bf16[1024,256]{1,0:T(8,128)(2,1)S(1)}, f32[2,1024]{1,0:T(2,128)S(1)}, f32[31,256]{1,0:T(8,128)S(1)}, f32[1,256]{1,0:T(1,128)S(1)}) custom-call(bf16[1024,256]{1,0:T(8,128)(2,1)} %value_hbm.1, bf16[1024,256]{1,0:T(8,128)(2,1)} %gate_hbm.1, f32[31,256]{1,0:T(8,128)} %taps_hbm.1, f32[1,256]{1,0:T(1,128)} %bitcast.2, ...), custom_call_target="tpu_custom_call" | custom-call | tf_op jit(solution)/shard_map/pallas_call | solution.py:521
  37.7 1.0 %shard_map.102 = (bf16[1024,256]{1,0:T(8,128)(2,1)}, bf16[1024,256]{1,0:T(8,128)(2,1)}, f32[2,1024]{1,0:T(2,128)}, f32[31,256]{1,0:T(8,128)}, f32[1,256]{1,0:T(1,128)}) custom-call(bf16[1024,256]{1,0:T(8,128)(2,1)S(1)} %get-tuple-element.15.refs_0_, bf16[1024,256]{1,0:T(8,128)(2,1)S(1)} %get-tuple-element.16.refs_1_, ...), custom_call_target="tpu_custom_call" | custom-call | tf_op jit(solution)/shard_map/pallas_call | solution.py:534

commit v6 on v5

--- a/solution.py
+++ b/solution.py
@@ -156,9 +156,9 @@
             total, square = total + v, square + v * v
         return row_sums(total), row_sums(square)
 
-    def conv_block(block):
+    def conv_block(block, halves=range(LANES // VB)):
         for lt in range(LT):
-            for half in range(LANES // VB):
+            for half in halves:
                 at = pl.multiple_of(block * LANES + half * VB, VB)
                 acc = jnp.zeros((VB, LANES), F32)
                 for k, window in windows(glu_s, lt, at + 2, VB):
@@ -170,25 +170,28 @@
     def stage1(block, _):
         sums = conv_stats(block)
 
-        conv_block(lax.rem(block + 1, NBLK))
+        conv_block(block + 1)
         record(ex1_src, ex1_rcv, block, sums)
-        for n, (first, size) in enumerate(chunks[:-1]):
+        for n, (first, size) in enumerate(chunks[:-2]):
 
             @pl.when(block == (first + size) // LANES - 1)
             def _(n=n):
                 exchange(ex1_src, ex1_rcv, ex1_sem, n)
 
-        @pl.when(block == NBLK - 2)
-        def _():
-            halo.wait_recv()
-            keep = jnp.where(sp == 0, 0.0, 1.0).astype(F32)
-            for lt in range(LT):
-                s = sigmoid(hv_s[1, :, lanes(lt)].astype(F32)) * keep
-                glu_s[lt, pl.ds(0, HALO), :] = hv_s[0, :, lanes(lt)].astype(F32) * s
-
         return 0
 
-    lax.fori_loop(1, NBLK, stage1, 0)
+    lax.fori_loop(1, NBLK - 1, stage1, 0)
+
+    sums = conv_stats(NBLK - 1)
+    conv_block(0, range(1, LANES // VB))
+    record(ex1_src, ex1_rcv, NBLK - 1, sums)
+    exchange(ex1_src, ex1_rcv, ex1_sem, len(chunks) - 2)
+    halo.wait_recv()
+    keep = jnp.where(sp == 0, 0.0, 1.0).astype(F32)
+    for lt in range(LT):
+        s = sigmoid(hv_s[1, :, lanes(lt)].astype(F32)) * keep
+        glu_s[lt, pl.ds(0, HALO), :] = hv_s[0, :, lanes(lt)].astype(F32) * s
+    conv_block(0, range(1))
     record(ex1_src, ex1_rcv, 0, conv_stats(0))
     exchange(ex1_src, ex1_rcv, ex1_sem, len(chunks) - 1)
 

time: 38.8 us -> 38.7 us (level)
  no operation moved by 1% of the time
where the time goes in v6:
time: 38.7 us; the launch traced here: 38.6 us
  Pallas kernels  37.9 us (98%)
  between operations  0.64 us (2%)
    pallas_call x1, Pallas kernels, per_device(): pl.pallas_call(functools.partial(kernel, params), out_shape=results, in_s...  36.9 us
    pallas_call x1, Pallas kernels, per_device(): pl.pallas_call(store_kernel, out_shape=results, in_specs=[vmem_spec] * 5,...  1.02 us

profile of v6, /device:TPU:1, one launch (start us, length us, event | category | flops | bytes accessed | tf_op | source)
XLA Modules:
  0.0 38.6 jit_solution(17740516844254822476)
XLA Ops:
  0.6 36.9 %shard_map.101 = (bf16[1024,256]{1,0:T(8,128)(2,1)S(1)}, bf16[1024,256]{1,0:T(8,128)(2,1)S(1)}, f32[2,1024]{1,0:T(2,128)S(1)}, f32[31,256]{1,0:T(8,128)S(1)}, f32[1,256]{1,0:T(1,128)S(1)}) custom-call(bf16[1024,256]{1,0:T(8,128)(2,1)} %value_hbm.1, bf16[1024,256]{1,0:T(8,128)(2,1)} %gate_hbm.1, f32[31,256]{1,0:T(8,128)} %taps_hbm.1, f32[1,256]{1,0:T(1,128)} %bitcast.2, ...), custom_call_target="tpu_custom_call" | custom-call | tf_op jit(solution)/shard_map/pallas_call | solution.py:524
  37.5 1.0 %shard_map.102 = (bf16[1024,256]{1,0:T(8,128)(2,1)}, bf16[1024,256]{1,0:T(8,128)(2,1)}, f32[2,1024]{1,0:T(2,128)}, f32[31,256]{1,0:T(8,128)}, f32[1,256]{1,0:T(1,128)}) custom-call(bf16[1024,256]{1,0:T(8,128)(2,1)S(1)} %get-tuple-element.15.refs_0_, bf16[1024,256]{1,0:T(8,128)(2,1)S(1)} %get-tuple-element.16.refs_1_, ...), custom_call_target="tpu_custom_call" | custom-call | tf_op jit(solution)/shard_map/pallas_call | solution.py:537
